TPU v7x, 256 devices: a whole 4x4x8 slice. The times are simulated.
256 devices in a mesh: fs: 32 (over z, x), tp: 8 (over y, core).
Axes of the slice: x: 4, y: 4, z: 8, core: 2. Of those that a mesh axis runs over, the one named last changes fastest.
Arguments:
- tokens: bfloat16 [4096, 2048], P('fs'), may hold values from -6 to 6
- route_ids: int32 [4096, 2], P('fs'), may hold values from 0 to 63, as said below
- route_weights: float32 [4096, 2], P('fs'), may hold values from 0.05 to 0.6
- norm_gain: float32 [2048], P('fs'), may hold values from 0.1 to 1.9
- gate_weight: float32 [64, 2048, 1024], P(None, 'fs', 'tp'), may hold values from -6 to 6
- up_weight: float32 [64, 2048, 1024], P(None, 'fs', 'tp'), may hold values from -6 to 6
- down_weight: float32 [64, 2048, 1024], P(None, 'fs', 'tp'), may hold values from -6 to 6
Outputs:
- gate_served: bfloat16 [64, 2048, 1024], P('fs', None, 'tp')
- up_served: bfloat16 [64, 2048, 1024], P('fs', None, 'tp')
- down_served: bfloat16 [64, 2048, 1024], P('fs', None, 'tp')
- combined: bfloat16 [4096, 2048], P('fs', 'tp')
Inputs may be any that keep to these rules, and one draw needn't show every extreme that they name: `route_ids`: each row names 2 different experts of one group, numbers g * 16 to g * 16 + 15 for some g. In each aligned block of 128 rows (the rows of one index of fs) no expert is named by more than 8 rows, and some experts are named by exactly 8 rows in every block.
All inputs are finite; a program needn't handle non-finite values.
Results may differ from a plain program's by a relative error of at most 0.015.
Values may be sent and summed in bfloat16 or wider, within the bound.
No kernel may reach another device: no remote copies, remote signals or barrier semaphores. Data moves between devices by JAX's collectives and lax.ppermute only.
A program may use at most 64 MiB of HBM per device.

v0:
```python
import jax
import jax.numpy as jnp
from jax import lax
from jax.experimental import pallas as pl
from jax.experimental.pallas import tpu as pltpu
from jax.sharding import Mesh
from jax.sharding import PartitionSpec as P

GROUPS = 4
TP = ("tp_0", "tp_1")
epsilon = 1e-06
BF16 = jnp.bfloat16
F32 = jnp.float32
MIB = 1024 * 1024


def exchange(blocks, axis):
    return lax.all_to_all(blocks, axis, split_axis=0, concat_axis=0, tiled=True)


def steps():
    return [(s, r) for s in range(lax.axis_size("tp_0")) for r in range(lax.axis_size("tp_1"))]


def moved(x, s, r):
    ny, nc = lax.axis_size("tp_0"), lax.axis_size("tp_1")
    pairs = [(y * nc + c, ((y + s) % ny) * nc + (c ^ r)) for y in range(ny) for c in range(nc)]
    return lax.ppermute(x, TP, pairs)


def spread_over_tp(blocks):
    y, c = lax.axis_index("tp_0"), lax.axis_index("tp_1")
    ny, nc = lax.axis_size("tp_0"), lax.axis_size("tp_1")
    result = []
    for s, r in steps():
        sent = lax.dynamic_index_in_dim(blocks, (y + s) % ny * nc + (c ^ r), 0, keepdims=False)
        result.append(sent if (s, r) == (0, 0) else moved(sent, s, r))
    return result


def gathered_over_tp(x):
    result = []
    for s in range(lax.axis_size("tp_0")):
        same = x if s == 0 else moved(x, s, 0)
        result += [same, moved(same, 0, 1)]
    return result


def prelude(tokens, route_ids, route_weights, down_weight, sources, n_tp):
    tok_rows, d_model = tokens.shape
    experts, rows_here, hidden_local = down_weight.shape
    per_device = experts // sources
    capacity = tok_rows * GROUPS // experts
    slots_out = per_device * capacity
    width = d_model // n_tp
    parts = 2
    dests = sources // parts
    slots = dests * slots_out

    def kernel(me_ref, tok_ref, own_ref, ids_ref, w_ref, down_ref, out_ref, weight_ref, own_scr):
        g = pl.program_id(0)

        @pl.when(g == 0)
        def _():
            x = tok_ref[...].astype(F32)
            inverse = lax.rsqrt(jnp.mean(x * x, axis=1, keepdims=True) + epsilon)
            own_scr[...] = (own_ref[...].astype(F32) * inverse).astype(BF16)

        slot = lax.broadcasted_iota(jnp.int32, (slots, tok_rows), 0) + g * slots
        expert_of, slot_of = slot // capacity, slot % capacity
        picks = [ids_ref[k : k + 1, :] == expert_of for k in range(ids_ref.shape[0])]
        named = picks[0]
        for p in picks[1:]:
            named = named | p
        row = lax.broadcasted_iota(jnp.int32, (tok_rows, tok_rows), 0)
        col = lax.broadcasted_iota(jnp.int32, (tok_rows, tok_rows), 1)
        earlier = jnp.where(row < col, 1.0, 0.0).astype(BF16)
        named_one = jnp.where(named, 1.0, 0.0).astype(BF16)
        before = jnp.dot(named_one, earlier, preferred_element_type=F32)
        here = named & (before == slot_of.astype(F32))
        here_one = jnp.where(here, 1.0, 0.0).astype(BF16)
        sent = jnp.dot(here_one, own_scr[...], preferred_element_type=F32).astype(BF16)
        out_ref[:, :slots_out, :] = sent.reshape(dests, slots_out, width)
        weight = jnp.zeros((slots, tok_rows), F32)
        for k, p in enumerate(picks):
            weight = weight + jnp.where(p & here, w_ref[k : k + 1, :], 0.0)
        weight_ref[...] = weight
        down = down_ref[...].astype(BF16).reshape(dests, per_device, rows_here, hidden_local)
        for e in range(per_device):
            out_ref[:, slots_out:, e * hidden_local : (e + 1) * hidden_local] = down[:, e]

    routes = route_ids.shape[1]
    grid = pltpu.PrefetchScalarGridSpec(
        num_scalar_prefetch=1,
        grid=(parts,),
        in_specs=[
            pl.BlockSpec((tok_rows, d_model), lambda g, me: (0, 0)),
            pl.BlockSpec((tok_rows, width), lambda g, me: (0, me[0])),
            pl.BlockSpec((routes, tok_rows), lambda g, me: (0, 0)),
            pl.BlockSpec((routes, tok_rows), lambda g, me: (0, 0)),
            pl.BlockSpec((dests * per_device, rows_here, hidden_local), lambda g, me: (g, 0, 0)),
        ],
        out_specs=[
            pl.BlockSpec((dests, slots_out + rows_here, width), lambda g, me: (g, 0, 0)),
            pl.BlockSpec((slots, tok_rows), lambda g, me: (g, 0)),
        ],
        scratch_shapes=[pltpu.VMEM((tok_rows, width), BF16)],
    )
    return pl.pallas_call(
        kernel,
        grid_spec=grid,
        out_shape=[
            pltpu.HBM((sources, slots_out + rows_here, width), BF16),
            pltpu.HBM((experts * capacity, tok_rows), F32),
        ],
        compiler_params=pltpu.CompilerParams(
            dimension_semantics=("arbitrary",), vmem_limit_bytes=12 * MIB
        ),
        name="prelude",
    )(
        lax.axis_index(TP).astype(jnp.int32).reshape(1),
        pltpu.with_memory_space_constraint(tokens, pltpu.HBM),
        pltpu.with_memory_space_constraint(tokens, pltpu.HBM),
        pltpu.with_memory_space_constraint(route_ids.T, pltpu.HBM),
        pltpu.with_memory_space_constraint(route_weights.T, pltpu.HBM),
        pltpu.with_memory_space_constraint(down_weight, pltpu.HBM),
    )


def hidden_units(pieces, both, per_device, capacity):
    sources, _, width = pieces[0].shape
    d_model, columns = both.shape
    slots = sources * capacity
    span = columns // per_device
    unit = span // 2
    order = steps()
    ny, nc = lax.axis_size("tp_0"), lax.axis_size("tp_1")

    def kernel(me_ref, both_ref, *refs):
        sources_ref, out_ref, held, sems = refs[: len(order)], refs[-3], refs[-2], refs[-1]
        copies = [
            pltpu.make_async_copy(piece, held.at[i], sems.at[i])
            for i, piece in enumerate(sources_ref)
        ]
        for copy in copies:
            copy.start()
        acc = [jnp.zeros((slots, span), F32) for _ in range(per_device)]
        for i, (s, r) in enumerate(order):
            copies[i].wait()
            block = lax.rem(me_ref[0] - s + ny, ny) * nc + (me_ref[1] if r == 0 else nc - 1 - me_ref[1])
            start = pl.multiple_of(block * width, width)
            for e in range(per_device):
                x = held[i, :, e * capacity : (e + 1) * capacity, :].reshape(slots, width)
                w = both_ref[pl.ds(start, width), e * span : (e + 1) * span]
                acc[e] = acc[e] + jnp.dot(x, w, preferred_element_type=F32)
        for e in range(per_device):
            pre = acc[e] * (d_model ** (-0.5))
            gate, up = pre[:, :unit], pre[:, unit:]
            out_ref[e * slots : (e + 1) * slots, :] = (gate / (1.0 + jnp.exp(-gate)) * up).astype(BF16)

    vmem = pl.BlockSpec(memory_space=pltpu.VMEM)
    me = jnp.stack([lax.axis_index("tp_0"), lax.axis_index("tp_1")]).astype(jnp.int32)
    return pl.pallas_call(
        kernel,
        in_specs=[pl.BlockSpec(memory_space=pltpu.SMEM), vmem]
        + [pl.BlockSpec(memory_space=pltpu.HBM)] * len(pieces),
        out_specs=vmem,
        scratch_shapes=[
            pltpu.VMEM((len(pieces), *pieces[0].shape), BF16),
            pltpu.SemaphoreType.DMA((len(pieces),)),
        ],
        out_shape=jax.ShapeDtypeStruct((per_device * slots, unit), BF16),
        compiler_params=pltpu.CompilerParams(vmem_limit_bytes=8 * MIB),
        name="hidden_units",
    )(me, both, *(pltpu.with_memory_space_constraint(p, pltpu.HBM) for p in pieces))


def down_projected(hidden, down, per_device, capacity, scale):
    rows, unit = hidden[0].shape
    width = down[0].shape[0]
    slots = rows // per_device
    sources = slots // capacity
    n = len(hidden)

    def kernel(*refs):
        h, d, out_ref = refs[:n], refs[n : 2 * n], refs[-1]
        for e in range(per_device):
            x = jnp.concatenate([ref[e * slots : (e + 1) * slots, :] for ref in h], axis=1)
            w = jnp.concatenate([ref[:, e * unit : (e + 1) * unit] for ref in d], axis=1)
            acc = lax.dot_general(x, w, (((1,), (1,)), ((), ())), preferred_element_type=F32)
            out_ref[:, e * capacity : (e + 1) * capacity, :] = (
                (acc * scale).astype(BF16).reshape(sources, capacity, width)
            )

    vmem = pl.BlockSpec(memory_space=pltpu.VMEM)
    return pl.pallas_call(
        kernel,
        in_specs=[vmem] * (2 * n),
        out_specs=vmem,
        out_shape=jax.ShapeDtypeStruct((sources, per_device * capacity, width), BF16),
        compiler_params=pltpu.CompilerParams(vmem_limit_bytes=8 * MIB),
        name="down_projected",
    )(*hidden, *down)


def work(tokens, route_ids, route_weights, norm_gain, gate_weight, up_weight, down_weight):
    tok_rows, d_model = tokens.shape
    experts, _, hidden_local = gate_weight.shape
    sources = lax.axis_size("fs")
    n_tp = lax.axis_size(TP)
    per_device = experts // sources
    capacity = tok_rows * GROUPS // experts
    col_width = d_model // n_tp
    slots_out = per_device * capacity

    first, weight = prelude(tokens, route_ids, route_weights, down_weight, sources, n_tp)
    first = exchange(first, "fs")

    scaling = norm_gain[None, :, None]
    folded = jnp.concatenate(
        [
            (scaling * w[e::per_device]).astype(BF16)
            for e in range(per_device)
            for w in (gate_weight, up_weight)
        ],
        axis=2,
    )
    folded, first = lax.optimization_barrier((folded, first))
    arrived = first[:, :slots_out]
    down_both = first[:, slots_out:].reshape(d_model, per_device * hidden_local)
    both = exchange(folded, "fs").reshape(d_model, 2 * per_device * hidden_local)

    down_tp = spread_over_tp(down_both.reshape(n_tp, col_width, per_device * hidden_local))
    pieces = gathered_over_tp(arrived)
    hidden = hidden_units(pieces, both, per_device, capacity)
    whole = gathered_over_tp(hidden)
    back = down_projected(whole, down_tp, per_device, capacity, (hidden_local * n_tp) ** (-0.5))
    back = exchange(back, "fs")
    back = back.reshape(experts * capacity, col_width).astype(F32)
    combined = lax.dot_general(
        weight, back, (((0,), (0,)), ((), ())), precision=lax.Precision.HIGHEST
    )
    parts = [both[:, i * hidden_local : (i + 1) * hidden_local] for i in range(2 * per_device)]
    down_served = jnp.stack(
        [down_both[:, e * hidden_local : (e + 1) * hidden_local] for e in range(per_device)]
    )
    return (jnp.stack(parts[0::2]), jnp.stack(parts[1::2]), down_served, combined.astype(BF16))


def solution(mesh):
    torus = Mesh(mesh.devices.reshape(mesh.shape["fs"], 4, 2), ("fs", "tp_0", "tp_1"))
    return jax.shard_map(
        work,
        mesh=torus,
        in_specs=(
            P("fs", None),
            P("fs", None),
            P("fs", None),
            P("fs"),
            P(None, "fs", TP),
            P(None, "fs", TP),
            P(None, "fs", TP),
        ),
        out_specs=(P("fs", None, TP), P("fs", None, TP), P("fs", None, TP), P("fs", TP)),
        check_vma=False,
    )
```

profile of v0, /device:TPU:32, one launch (start us, length us, event | category | flops | bytes accessed | tf_op | source)
XLA Modules:
  0.0 140.0 jit_solution(12700337003983293567)
XLA Ops:
  0.6 3.2 %prelude.1 = (bf16[32,80,256]{2,1,0:T(8,128)(2,1)}, f32[512,128]{1,0:T(8,128)}) custom-call(s32[1]{0:T(128)} %bitcast.me_ref, bf16[128,2048]{1,0:T(8,128)(2,1)} %own_ref.1, bf16[128,2048]{1,0:T(8,128)(2,1)} %own_ref.1, s32[2,128]{1,0:T(2,128)} %bitcast.44, f32[2,128]{1,0:T(2,128)} %bitcast.45, f32[64,64,128]{2,1,0:T(8,128)} %down_ref.1), custom_call_target="tpu_custom_call" | custom-call | tf_op jit(solution)/shard_map/prelude/pallas_call | solution.py:109
  3.8 11.3 %all-to-all-start = ((bf16[32,80,256]{2,1,0:T(8,128)(2,1)}), bf16[32,80,256]{2,1,0:T(8,128)(2,1)S(1)}, u32[]{:S(2)}, u32[]{:S(2)}) async-start(bf16[32,80,256]{2,1,0:T(8,128)(2,1)} %get-tuple-element.8), calls=%async_computation | async-start | bytes 2621440 | tf_op jit(solution)/shard_map/all_to_all | solution.py:18
  15.2 2.2 %multiply_convert_fusion.3 = (bf16[32,64,128]{2,1,0:T(8,128)(2,1)S(1)}, bf16[32,64,128]{2,1,0:T(8,128)(2,1)S(1)}, bf16[32,64,128]{2,1,0:T(8,128)(2,1)S(1)}, bf16[32,64,128]{2,1,0:T(8,128)(2,1)S(1)}) fusion(f32[64,64,128]{2,1,0:T(8,128)S(1)} %copy-done.2, f32[64]{0:T(128)S(1)} %copy-done.6, f32[64,64,128]{2,1,0:T(8,128)} %param.12), kind=kLoop, calls=%fused_computation.8 | loop fusion | flops 2097152 | bytes 6291712 | tf_op jit(solution)/shard_map/convert_element_type | solution.py:222
  17.4 1.6 %pad_maximum_fusion = bf16[32,64,512]{2,1,0:T(8,128)(2,1)} fusion(bf16[32,64,128]{2,1,0:T(8,128)(2,1)S(1)} %get-tuple-element.30, bf16[32,64,128]{2,1,0:T(8,128)(2,1)S(1)} %get-tuple-element.13, bf16[32,64,128]{2,1,0:T(8,128)(2,1)S(1)} %get-tuple-element.31, bf16[32,64,128]{2,1,0:T(8,128)(2,1)S(1)} %get-tuple-element.12), kind=kLoop, calls=%fused_computation | loop fusion | flops 8388608 | bytes 4194304 | tf_op jit(solution)/shard_map/concatenate | solution.py:220
  19.0 28.9 %all-to-all-done = bf16[32,80,256]{2,1,0:T(8,128)(2,1)S(1)} async-done(((bf16[32,80,256]{2,1,0:T(8,128)(2,1)}), bf16[32,80,256]{2,1,0:T(8,128)(2,1)S(1)}, u32[]{:S(2)}, u32[]{:S(2)}) %all-to-all-start) | async-done | bytes 1310752 | tf_op jit(solution)/shard_map/all_to_all | solution.py:18
  48.0 6.5 %all-to-all-start.1 = ((bf16[32,64,512]{2,1,0:T(8,128)(2,1)}), bf16[32,64,512]{2,1,0:T(8,128)(2,1)S(1)}, u32[]{:S(2)}, u32[]{:S(2)}) async-start(bf16[32,64,512]{2,1,0:T(8,128)(2,1)} %pad_maximum_fusion), calls=%async_computation.1 | async-start | bytes 4194304 | tf_op jit(solution)/shard_map/all_to_all | solution.py:18
  54.4 0.7 slice.47.refs_0_
  55.2 3.0 %collective-permute-start.5 = (bf16[32,16,256]{2,1,0:T(8,128)(2,1)}, bf16[32,16,256]{2,1,0:T(8,128)(2,1)}, u32[]{:S(2)}, u32[]{:S(2)}) collective-permute-start(bf16[32,16,256]{2,1,0:T(8,128)(2,1)} %slice.47.refs_0_), channel_id=1, source_target_pairs={{0,6},{1,7},{2,0},{3,1},{4,2},{5,3},{6,4},{7,5},{8,14},{9,15},{10,... | collective-permute-start | bytes 786440 | tf_op jit(solution)/shard_map/ppermute | solution.py:28
  58.2 0.6 collective-permute-start.3
  58.8 1.0 collective-permute-start.1
  59.8 0.0 collective-permute-start
  59.8 8.3 %collective-permute-done.5.refs_6_ = bf16[32,16,256]{2,1,0:T(8,128)(2,1)} collective-permute-done((bf16[32,16,256]{2,1,0:T(8,128)(2,1)}, bf16[32,16,256]{2,1,0:T(8,128)(2,1)}, u32[]{:S(2)}, u32[]{:S(2)}) %collective-permute-start.5) | collective-permute-done | bytes 262176 | tf_op jit(solution)/shard_map/ppermute | solution.py:28
  68.0 0.0 collective-permute-start.6
  68.0 0.9 collective-permute-done.3.refs_4_
  69.0 0.1 slice.44
  69.1 0.0 copy-start
  69.1 2.6 %collective-permute-done.1.refs_2_ = bf16[32,16,256]{2,1,0:T(8,128)(2,1)} collective-permute-done((bf16[32,16,256]{2,1,0:T(8,128)(2,1)}, bf16[32,16,256]{2,1,0:T(8,128)(2,1)}, u32[]{:S(2)}, u32[]{:S(2)}) %collective-permute-start.1) | collective-permute-done | bytes 262176 | tf_op jit(solution)/shard_map/ppermute | solution.py:28
  71.8 0.9 dynamic-slice_bitcast_fusion
  72.6 0.9 collective-permute-start.20
  73.5 0.0 collective-permute-done.refs_1_
  73.5 0.4 collective-permute-start.19
  73.9 0.0 collective-permute-done.6.refs_7_
  73.9 2.2 %collective-permute-start.18 = (bf16[256,256]{1,0:T(8,128)(2,1)}, bf16[256,256]{1,0:T(8,128)(2,1)S(1)}, u32[]{:S(2)}, u32[]{:S(2)}) collective-permute-start(bf16[256,256]{1,0:T(8,128)(2,1)} %get-tuple-element.22), channel_id=1, source_target_pairs={{0,5},{1,4},{2,7},{3,6},{4,1},{5,0},{6,3},{7,2},{8,13},{9,12},{10,... | collective-permute-start | bytes 393224 | tf_op jit(solution)/shard_map/ppermute | solution.py:28
  76.2 0.0 collective-permute-done.4.refs_5_
  76.2 0.8 collective-permute-start.17
  77.0 0.1 pad_add_fusion.me_ref
  77.0 0.0 collective-permute-done.2.refs_3_
  77.0 1.6 %collective-permute-start.16 = (bf16[256,256]{1,0:T(8,128)(2,1)}, bf16[256,256]{1,0:T(8,128)(2,1)S(1)}, u32[]{:S(2)}, u32[]{:S(2)}) collective-permute-start(bf16[256,256]{1,0:T(8,128)(2,1)} %get-tuple-element.24), channel_id=1, source_target_pairs={{0,3},{1,2},{2,5},{3,4},{4,7},{5,6},{6,1},{7,0},{8,11},{9,10},{10,... | collective-permute-start | bytes 393224 | tf_op jit(solution)/shard_map/ppermute | solution.py:28
  78.7 24.4 %all-to-all-done.1 = bf16[32,64,512]{2,1,0:T(8,128)(2,1)S(1)} async-done(((bf16[32,64,512]{2,1,0:T(8,128)(2,1)}), bf16[32,64,512]{2,1,0:T(8,128)(2,1)S(1)}, u32[]{:S(2)}, u32[]{:S(2)}) %all-to-all-start.1) | async-done | bytes 2097184 | tf_op jit(solution)/shard_map/all_to_all | solution.py:18
  103.0 2.7 %hidden_units.1.refs_0_ = bf16[512,128]{1,0:T(8,128)(2,1)S(1)} custom-call(s32[2]{0:T(128)S(1)} %pad_add_fusion.me_ref, bf16[2048,512]{1,0:T(8,128)(2,1)S(1)} %bitcast.39, bf16[32,16,256]{2,1,0:T(8,128)(2,1)} %slice.47.refs_0_, bf16[32,16,256]{2,1,0:T(8,128)(2,1)} %collective-permute-done.refs_1_, bf16[32,16,256]{2,1,0:T(8,128)(2,1)} %collective-permute-done.1.refs_2_, ...), custom_call_target="tpu_custom_call" | custom-call | tf_op jit(solution)/shard_map/hidden_units/pallas_call | solution.py:163
  105.7 1.6 %collective-permute-start.15 = (bf16[256,256]{1,0:T(8,128)(2,1)S(1)}, bf16[256,256]{1,0:T(8,128)(2,1)S(1)}, u32[]{:S(2)}, u32[]{:S(2)}) collective-permute-start(bf16[256,256]{1,0:T(8,128)(2,1)S(1)} %copy-done.5), channel_id=1, source_target_pairs={{0,2},{1,3},{2,4},{3,5},{4,6},{5,7},{6,0},{7,1},{8,10},{9,11},{10,... | collective-permute-start | bytes 393224 | tf_op jit(solution)/shard_map/ppermute | solution.py:28
  107.4 1.7 %collective-permute-start.12 = (bf16[512,128]{1,0:T(8,128)(2,1)S(1)}, bf16[512,128]{1,0:T(8,128)(2,1)S(1)}, u32[]{:S(2)}, u32[]{:S(2)}) collective-permute-start(bf16[512,128]{1,0:T(8,128)(2,1)S(1)} %hidden_units.1.refs_0_), channel_id=1, source_target_pairs={{0,6},{1,7},{2,0},{3,1},{4,2},{5,3},{6,4},{7,5},{8,14},{9,15},{10,... | collective-permute-start | bytes 393224 | tf_op jit(solution)/shard_map/ppermute | solution.py:28
  109.1 1.9 %collective-permute-start.10 = (bf16[512,128]{1,0:T(8,128)(2,1)S(1)}, bf16[512,128]{1,0:T(8,128)(2,1)S(1)}, u32[]{:S(2)}, u32[]{:S(2)}) collective-permute-start(bf16[512,128]{1,0:T(8,128)(2,1)S(1)} %hidden_units.1.refs_0_), channel_id=1, source_target_pairs={{0,4},{1,5},{2,6},{3,7},{4,0},{5,1},{6,2},{7,3},{8,12},{9,13},{10,... | collective-permute-start | bytes 393224 | tf_op jit(solution)/shard_map/ppermute | solution.py:28
  111.0 0.7 collective-permute-start.8
  111.7 0.1 slice_bitcast_fusion.1
  111.8 0.1 collective-permute-start.14
  111.9 1.5 %collective-permute-done.15.refs_10_ = bf16[256,256]{1,0:T(8,128)(2,1)S(1)} collective-permute-done((bf16[256,256]{1,0:T(8,128)(2,1)S(1)}, bf16[256,256]{1,0:T(8,128)(2,1)S(1)}, u32[]{:S(2)}, u32[]{:S(2)}) %collective-permute-start.15) | collective-permute-done | bytes 131104 | tf_op jit(solution)/shard_map/ppermute | solution.py:28
  113.4 0.5 collective-permute-start.13
  113.9 1.6 %collective-permute-done.10.refs_4_ = bf16[512,128]{1,0:T(8,128)(2,1)S(1)} collective-permute-done((bf16[512,128]{1,0:T(8,128)(2,1)S(1)}, bf16[512,128]{1,0:T(8,128)(2,1)S(1)}, u32[]{:S(2)}, u32[]{:S(2)}) %collective-permute-start.10) | collective-permute-done | bytes 131104 | tf_op jit(solution)/shard_map/ppermute | solution.py:28
  115.6 1.6 %collective-permute-done.8.refs_2_ = bf16[512,128]{1,0:T(8,128)(2,1)S(1)} collective-permute-done((bf16[512,128]{1,0:T(8,128)(2,1)S(1)}, bf16[512,128]{1,0:T(8,128)(2,1)S(1)}, u32[]{:S(2)}, u32[]{:S(2)}) %collective-permute-start.8) | collective-permute-done | bytes 131104 | tf_op jit(solution)/shard_map/ppermute | solution.py:28
  117.2 1.1 pad_maximum_fusion.3
  118.3 0.3 collective-permute-done.9.refs_3_
  118.5 1.2 down_projected.1
  119.7 6.7 %all-to-all-start.2 = ((bf16[32,16,256]{2,1,0:T(8,128)(2,1)}), bf16[32,16,256]{2,1,0:T(8,128)(2,1)S(1)}, u32[]{:S(2)}, u32[]{:S(2)}) async-start(bf16[32,16,256]{2,1,0:T(8,128)(2,1)} %down_projected.1), calls=%async_computation.2 | async-start | bytes 524288 | tf_op jit(solution)/shard_map/all_to_all | solution.py:18
  126.4 0.4 slice_bitcast_fusion.3
  126.8 1.5 %pad_maximum_fusion.1 = (bf16[2,2048,128]{2,1,0:T(8,128)(2,1)}, bf16[2,2048,128]{2,1,0:T(8,128)(2,1)}) fusion(bf16[1,2048,128]{2,1,0:T(8,128)(2,1)S(1)} %get-tuple-element.18, bf16[1,2048,128]{2,1,0:T(8,128)(2,1)S(1)} %get-tuple-element.19, bf16[1,2048,128]{2,1,0:T(8,128)(2,1)S(1)} %get-tuple-element.17, bf16[1,2048,128]{2,1,0:T(8,128)(2,1)S(1)} %get-tuple-element.16), kind=kLoop, calls=%fused_computation.2 | loop fusion | flops 1048576 | bytes 4194304 | tf_op jit(solution)/shard_map/stack | solution.py:247
  128.3 10.7 %all-to-all-done.2 = bf16[32,16,256]{2,1,0:T(8,128)(2,1)S(1)} async-done(((bf16[32,16,256]{2,1,0:T(8,128)(2,1)}), bf16[32,16,256]{2,1,0:T(8,128)(2,1)S(1)}, u32[]{:S(2)}, u32[]{:S(2)}) %all-to-all-start.2) | async-done | bytes 262176 | tf_op jit(solution)/shard_map/all_to_all | solution.py:18
  139.0 1.0 convolution_convert_fusion
  (28 shorter events, 0.1 us)
Async XLA Ops:
  3.8 11.4 %copy-start.2 = (f32[64,64,128]{2,1,0:T(8,128)S(1)}, f32[64,64,128]{2,1,0:T(8,128)}, u32[]{:S(2)}) copy-start(f32[64,64,128]{2,1,0:T(8,128)} %param.11) | copy-start | bytes 6291460
  3.8 11.4 %copy-start.6 = (f32[64]{0:T(128)S(1)}, f32[64]{0:T(128)}, u32[]{:S(2)}) copy-start(f32[64]{0:T(128)} %param.10) | copy-start | bytes 772
  3.8 44.1 %all-to-all-start = ((bf16[32,80,256]{2,1,0:T(8,128)(2,1)}), bf16[32,80,256]{2,1,0:T(8,128)(2,1)S(1)}, u32[]{:S(2)}, u32[]{:S(2)}) async-start(bf16[32,80,256]{2,1,0:T(8,128)(2,1)} %get-tuple-element.8), calls=%async_computation | async-start | bytes 2621440 | tf_op jit(solution)/shard_map/all_to_all | solution.py:18
  48.0 55.0 %all-to-all-start.1 = ((bf16[32,64,512]{2,1,0:T(8,128)(2,1)}), bf16[32,64,512]{2,1,0:T(8,128)(2,1)S(1)}, u32[]{:S(2)}, u32[]{:S(2)}) async-start(bf16[32,64,512]{2,1,0:T(8,128)(2,1)} %pad_maximum_fusion), calls=%async_computation.1 | async-start | bytes 4194304 | tf_op jit(solution)/shard_map/all_to_all | solution.py:18
  55.2 12.9 %collective-permute-start.5 = (bf16[32,16,256]{2,1,0:T(8,128)(2,1)}, bf16[32,16,256]{2,1,0:T(8,128)(2,1)}, u32[]{:S(2)}, u32[]{:S(2)}) collective-permute-start(bf16[32,16,256]{2,1,0:T(8,128)(2,1)} %slice.47.refs_0_), channel_id=1, source_target_pairs={{0,6},{1,7},{2,0},{3,1},{4,2},{5,3},{6,4},{7,5},{8,14},{9,15},{10,... | collective-permute-start | bytes 786440 | tf_op jit(solution)/shard_map/ppermute | solution.py:28
  58.2 10.8 %collective-permute-start.3 = (bf16[32,16,256]{2,1,0:T(8,128)(2,1)}, bf16[32,16,256]{2,1,0:T(8,128)(2,1)}, u32[]{:S(2)}, u32[]{:S(2)}) collective-permute-start(bf16[32,16,256]{2,1,0:T(8,128)(2,1)} %slice.47.refs_0_), channel_id=1, source_target_pairs={{0,4},{1,5},{2,6},{3,7},{4,0},{5,1},{6,2},{7,3},{8,12},{9,13},{10,... | collective-permute-start | bytes 786440 | tf_op jit(solution)/shard_map/ppermute | solution.py:28
  58.8 12.9 %collective-permute-start.1 = (bf16[32,16,256]{2,1,0:T(8,128)(2,1)}, bf16[32,16,256]{2,1,0:T(8,128)(2,1)}, u32[]{:S(2)}, u32[]{:S(2)}) collective-permute-start(bf16[32,16,256]{2,1,0:T(8,128)(2,1)} %slice.47.refs_0_), channel_id=1, source_target_pairs={{0,2},{1,3},{2,4},{3,5},{4,6},{5,7},{6,0},{7,1},{8,10},{9,11},{10,... | collective-permute-start | bytes 786440 | tf_op jit(solution)/shard_map/ppermute | solution.py:28
  59.8 13.7 %collective-permute-start = (bf16[32,16,256]{2,1,0:T(8,128)(2,1)}, bf16[32,16,256]{2,1,0:T(8,128)(2,1)}, u32[]{:S(2)}, u32[]{:S(2)}) collective-permute-start(bf16[32,16,256]{2,1,0:T(8,128)(2,1)} %slice.47.refs_0_), channel_id=1, source_target_pairs={{0,1},{1,0},{2,3},{3,2},{4,5},{5,4},{6,7},{7,6},{8,9},{9,8},{10,11... | collective-permute-start | bytes 786440 | tf_op jit(solution)/shard_map/ppermute | solution.py:28
  68.0 5.9 %collective-permute-start.6 = (bf16[32,16,256]{2,1,0:T(8,128)(2,1)}, bf16[32,16,256]{2,1,0:T(8,128)(2,1)}, u32[]{:S(2)}, u32[]{:S(2)}) collective-permute-start(bf16[32,16,256]{2,1,0:T(8,128)(2,1)} %collective-permute-done.5.refs_6_), channel_id=1, source_target_pairs={{0,1},{1,0},{2,3},{3,2},{4,5},{5,4},{6,7},{7,6},{8,9},{9,8},{10,11... | collective-permute-start | bytes 786440 | tf_op jit(solution)/shard_map/ppermute | solution.py:28
  69.0 7.2 %collective-permute-start.4 = (bf16[32,16,256]{2,1,0:T(8,128)(2,1)}, bf16[32,16,256]{2,1,0:T(8,128)(2,1)}, u32[]{:S(2)}, u32[]{:S(2)}) collective-permute-start(bf16[32,16,256]{2,1,0:T(8,128)(2,1)} %collective-permute-done.3.refs_4_), channel_id=1, source_target_pairs={{0,1},{1,0},{2,3},{3,2},{4,5},{5,4},{6,7},{7,6},{8,9},{9,8},{10,11... | collective-permute-start | bytes 786440 | tf_op jit(solution)/shard_map/ppermute | solution.py:28
  69.1 7.9 %copy-start = (bf16[32,64,256]{2,1,0:T(8,128)(2,1)}, bf16[32,64,256]{2,1,0:T(8,128)(2,1)S(1)}, u32[]{:S(2)}) copy-start(bf16[32,64,256]{2,1,0:T(8,128)(2,1)S(1)} %slice.44) | copy-start | bytes 3145732
  71.8 5.3 %collective-permute-start.2 = (bf16[32,16,256]{2,1,0:T(8,128)(2,1)}, bf16[32,16,256]{2,1,0:T(8,128)(2,1)S(1)}, u32[]{:S(2)}, u32[]{:S(2)}) collective-permute-start(bf16[32,16,256]{2,1,0:T(8,128)(2,1)} %collective-permute-done.1.refs_2_), channel_id=1, source_target_pairs={{0,1},{1,0},{2,3},{3,2},{4,5},{5,4},{6,7},{7,6},{8,9},{9,8},{10,11... | collective-permute-start | bytes 786440 | tf_op jit(solution)/shard_map/ppermute | solution.py:28
  72.6 33.1 %collective-permute-start.20 = (bf16[256,256]{1,0:T(8,128)(2,1)}, bf16[256,256]{1,0:T(8,128)(2,1)S(1)}, u32[]{:S(2)}, u32[]{:S(2)}) collective-permute-start(bf16[256,256]{1,0:T(8,128)(2,1)} %get-tuple-element.20), channel_id=1, source_target_pairs={{0,7},{1,6},{2,1},{3,0},{4,3},{5,2},{6,5},{7,4},{8,15},{9,14},{10,... | collective-permute-start | bytes 393224 | tf_op jit(solution)/shard_map/ppermute | solution.py:28
  73.5 33.9 %collective-permute-start.19 = (bf16[256,256]{1,0:T(8,128)(2,1)}, bf16[256,256]{1,0:T(8,128)(2,1)S(1)}, u32[]{:S(2)}, u32[]{:S(2)}) collective-permute-start(bf16[256,256]{1,0:T(8,128)(2,1)} %get-tuple-element.21), channel_id=1, source_target_pairs={{0,6},{1,7},{2,0},{3,1},{4,2},{5,3},{6,4},{7,5},{8,14},{9,15},{10,... | collective-permute-start | bytes 393224 | tf_op jit(solution)/shard_map/ppermute | solution.py:28
  73.9 35.1 %collective-permute-start.18 = (bf16[256,256]{1,0:T(8,128)(2,1)}, bf16[256,256]{1,0:T(8,128)(2,1)S(1)}, u32[]{:S(2)}, u32[]{:S(2)}) collective-permute-start(bf16[256,256]{1,0:T(8,128)(2,1)} %get-tuple-element.22), channel_id=1, source_target_pairs={{0,5},{1,4},{2,7},{3,6},{4,1},{5,0},{6,3},{7,2},{8,13},{9,12},{10,... | collective-permute-start | bytes 393224 | tf_op jit(solution)/shard_map/ppermute | solution.py:28
  76.2 34.8 %collective-permute-start.17 = (bf16[256,256]{1,0:T(8,128)(2,1)}, bf16[256,256]{1,0:T(8,128)(2,1)S(1)}, u32[]{:S(2)}, u32[]{:S(2)}) collective-permute-start(bf16[256,256]{1,0:T(8,128)(2,1)} %get-tuple-element.23), channel_id=1, source_target_pairs={{0,4},{1,5},{2,6},{3,7},{4,0},{5,1},{6,2},{7,3},{8,12},{9,13},{10,... | collective-permute-start | bytes 393224 | tf_op jit(solution)/shard_map/ppermute | solution.py:28
  77.0 26.0 %copy-start.3 = (bf16[32,16,256]{2,1,0:T(8,128)(2,1)}, bf16[32,16,256]{2,1,0:T(8,128)(2,1)S(1)}, u32[]{:S(2)}) copy-start(bf16[32,16,256]{2,1,0:T(8,128)(2,1)S(1)} %collective-permute-done.2.refs_3_) | copy-start | bytes 786436
  77.0 34.7 %collective-permute-start.16 = (bf16[256,256]{1,0:T(8,128)(2,1)}, bf16[256,256]{1,0:T(8,128)(2,1)S(1)}, u32[]{:S(2)}, u32[]{:S(2)}) collective-permute-start(bf16[256,256]{1,0:T(8,128)(2,1)} %get-tuple-element.24), channel_id=1, source_target_pairs={{0,3},{1,2},{2,5},{3,4},{4,7},{5,6},{6,1},{7,0},{8,11},{9,10},{10,... | collective-permute-start | bytes 393224 | tf_op jit(solution)/shard_map/ppermute | solution.py:28
  103.0 2.7 %copy-start.5 = (bf16[256,256]{1,0:T(8,128)(2,1)S(1)}, bf16[256,256]{1,0:T(8,128)(2,1)}, u32[]{:S(2)}) copy-start(bf16[256,256]{1,0:T(8,128)(2,1)} %get-tuple-element.25) | copy-start | bytes 393220
  103.0 8.7 %copy-start.1 = (bf16[32,64,256]{2,1,0:T(8,128)(2,1)S(1)}, bf16[32,64,256]{2,1,0:T(8,128)(2,1)}, u32[]{:S(2)}) copy-start(bf16[32,64,256]{2,1,0:T(8,128)(2,1)} %copy-done) | copy-start | bytes 3145732
  105.7 7.7 %collective-permute-start.15 = (bf16[256,256]{1,0:T(8,128)(2,1)S(1)}, bf16[256,256]{1,0:T(8,128)(2,1)S(1)}, u32[]{:S(2)}, u32[]{:S(2)}) collective-permute-start(bf16[256,256]{1,0:T(8,128)(2,1)S(1)} %copy-done.5), channel_id=1, source_target_pairs={{0,2},{1,3},{2,4},{3,5},{4,6},{5,7},{6,0},{7,1},{8,10},{9,11},{10,... | collective-permute-start | bytes 393224 | tf_op jit(solution)/shard_map/ppermute | solution.py:28
  107.4 6.0 %collective-permute-start.12 = (bf16[512,128]{1,0:T(8,128)(2,1)S(1)}, bf16[512,128]{1,0:T(8,128)(2,1)S(1)}, u32[]{:S(2)}, u32[]{:S(2)}) collective-permute-start(bf16[512,128]{1,0:T(8,128)(2,1)S(1)} %hidden_units.1.refs_0_), channel_id=1, source_target_pairs={{0,6},{1,7},{2,0},{3,1},{4,2},{5,3},{6,4},{7,5},{8,14},{9,15},{10,... | collective-permute-start | bytes 393224 | tf_op jit(solution)/shard_map/ppermute | solution.py:28
  109.1 6.5 %collective-permute-start.10 = (bf16[512,128]{1,0:T(8,128)(2,1)S(1)}, bf16[512,128]{1,0:T(8,128)(2,1)S(1)}, u32[]{:S(2)}, u32[]{:S(2)}) collective-permute-start(bf16[512,128]{1,0:T(8,128)(2,1)S(1)} %hidden_units.1.refs_0_), channel_id=1, source_target_pairs={{0,4},{1,5},{2,6},{3,7},{4,0},{5,1},{6,2},{7,3},{8,12},{9,13},{10,... | collective-permute-start | bytes 393224 | tf_op jit(solution)/shard_map/ppermute | solution.py:28
  111.0 6.2 %collective-permute-start.8 = (bf16[512,128]{1,0:T(8,128)(2,1)S(1)}, bf16[512,128]{1,0:T(8,128)(2,1)S(1)}, u32[]{:S(2)}, u32[]{:S(2)}) collective-permute-start(bf16[512,128]{1,0:T(8,128)(2,1)S(1)} %hidden_units.1.refs_0_), channel_id=1, source_target_pairs={{0,2},{1,3},{2,4},{3,5},{4,6},{5,7},{6,0},{7,1},{8,10},{9,11},{10,... | collective-permute-start | bytes 393224 | tf_op jit(solution)/shard_map/ppermute | solution.py:28
  111.8 6.5 %collective-permute-start.14 = (bf16[256,256]{1,0:T(8,128)(2,1)S(1)}, bf16[256,256]{1,0:T(8,128)(2,1)S(1)}, u32[]{:S(2)}, u32[]{:S(2)}) collective-permute-start(bf16[256,256]{1,0:T(8,128)(2,1)S(1)} %get-tuple-element.26), channel_id=1, source_target_pairs={{0,1},{1,0},{2,3},{3,2},{4,5},{5,4},{6,7},{7,6},{8,9},{9,8},{10,11... | collective-permute-start | bytes 393224 | tf_op jit(solution)/shard_map/ppermute | solution.py:28
  113.4 4.9 %collective-permute-start.7 = (bf16[512,128]{1,0:T(8,128)(2,1)S(1)}, bf16[512,128]{1,0:T(8,128)(2,1)S(1)}, u32[]{:S(2)}, u32[]{:S(2)}) collective-permute-start(bf16[512,128]{1,0:T(8,128)(2,1)S(1)} %hidden_units.1.refs_0_), channel_id=1, source_target_pairs={{0,1},{1,0},{2,3},{3,2},{4,5},{5,4},{6,7},{7,6},{8,9},{9,8},{10,11... | collective-permute-start | bytes 393224 | tf_op jit(solution)/shard_map/ppermute | solution.py:28
  113.4 4.8 %collective-permute-start.13 = (bf16[512,128]{1,0:T(8,128)(2,1)S(1)}, bf16[512,128]{1,0:T(8,128)(2,1)S(1)}, u32[]{:S(2)}, u32[]{:S(2)}) collective-permute-start(bf16[512,128]{1,0:T(8,128)(2,1)S(1)} %collective-permute-done.12.refs_6_), channel_id=1, source_target_pairs={{0,1},{1,0},{2,3},{3,2},{4,5},{5,4},{6,7},{7,6},{8,9},{9,8},{10,11... | collective-permute-start | bytes 393224 | tf_op jit(solution)/shard_map/ppermute | solution.py:28
  115.6 2.7 %collective-permute-start.11 = (bf16[512,128]{1,0:T(8,128)(2,1)S(1)}, bf16[512,128]{1,0:T(8,128)(2,1)S(1)}, u32[]{:S(2)}, u32[]{:S(2)}) collective-permute-start(bf16[512,128]{1,0:T(8,128)(2,1)S(1)} %collective-permute-done.10.refs_4_), channel_id=1, source_target_pairs={{0,1},{1,0},{2,3},{3,2},{4,5},{5,4},{6,7},{7,6},{8,9},{9,8},{10,11... | collective-permute-start | bytes 393224 | tf_op jit(solution)/shard_map/ppermute | solution.py:28
  117.2 1.3 collective-permute-start.9
  119.7 19.3 %all-to-all-start.2 = ((bf16[32,16,256]{2,1,0:T(8,128)(2,1)}), bf16[32,16,256]{2,1,0:T(8,128)(2,1)S(1)}, u32[]{:S(2)}, u32[]{:S(2)}) async-start(bf16[32,16,256]{2,1,0:T(8,128)(2,1)} %down_projected.1), calls=%async_computation.2 | async-start | bytes 524288 | tf_op jit(solution)/shard_map/all_to_all | solution.py:18
  126.8 12.2 %copy-start.4 = (f32[512,128]{1,0:T(8,128)S(1)}, f32[512,128]{1,0:T(8,128)}, u32[]{:S(2)}) copy-start(f32[512,128]{1,0:T(8,128)} %get-tuple-element.11) | copy-start | bytes 786436
where the time goes:
time: 141 us; the launch traced here: 140 us
  waiting for transfers between devices  80.9 us (57%)
  starting transfers between devices  41.6 us (30%)
  Pallas kernels  7.03 us (5%)
  other arithmetic  6.47 us (5%)
  local copies, waits for them, and re-layouts  2.19 us (2%)
    all_to_all x3, waiting for transfers between devices, exchange(): return lax.all_to_all(blocks, axis, split_axis=0, concat_axis=0, tiled=True)  64 us
    all_to_all x3, starting transfers between devices, exchange(): return lax.all_to_all(blocks, axis, split_axis=0, concat_axis=0, tiled=True)  24.5 us
    ppermute x21, starting transfers between devices, moved(): return lax.ppermute(x, TP, pairs)  17.1 us
    ppermute x21, waiting for transfers between devices, moved(): return lax.ppermute(x, TP, pairs)  16.9 us
    pallas_call x1, Pallas kernels, prelude(): pl.pallas_call(kernel, grid_spec=grid, out_shape=[pltpu.HBM((sources, slo...  3.19 us
  transfers between devices with their start and end apart: 24, of which 10 were waited for; matrix products, arithmetic and copies ran while one was open for 6% of the time, Pallas kernels for 2%

commit v1 on v0

--- a/solution.py
+++ b/solution.py
@@ -12,6 +12,7 @@
 BF16 = jnp.bfloat16
 F32 = jnp.float32
 MIB = 1024 * 1024
+FS_SHAPE = (8, 4)
 
 
 def exchange(blocks, axis):
@@ -127,16 +128,19 @@
     )
 
 
-def hidden_units(pieces, both, per_device, capacity):
+def hidden_units(pieces, top, rest, per_device, capacity):
     sources, _, width = pieces[0].shape
-    d_model, columns = both.shape
+    columns = top.shape[2]
+    rows_here = top.shape[1] + rest.shape[1]
+    d_model = sources * rows_here
+    across = width // rows_here
     slots = sources * capacity
     span = columns // per_device
     unit = span // 2
     order = steps()
     ny, nc = lax.axis_size("tp_0"), lax.axis_size("tp_1")
 
-    def kernel(me_ref, both_ref, *refs):
+    def kernel(me_ref, top_ref, rest_ref, *refs):
         sources_ref, out_ref, held, sems = refs[: len(order)], refs[-3], refs[-2], refs[-1]
         copies = [
             pltpu.make_async_copy(piece, held.at[i], sems.at[i])
@@ -148,10 +152,12 @@
         for i, (s, r) in enumerate(order):
             copies[i].wait()
             block = lax.rem(me_ref[0] - s + ny, ny) * nc + (me_ref[1] if r == 0 else nc - 1 - me_ref[1])
-            start = pl.multiple_of(block * width, width)
+            here = pl.ds(block * across, across)
             for e in range(per_device):
                 x = held[i, :, e * capacity : (e + 1) * capacity, :].reshape(slots, width)
-                w = both_ref[pl.ds(start, width), e * span : (e + 1) * span]
+                w = jnp.concatenate(
+                    [ref[here, :, e * span : (e + 1) * span] for ref in (top_ref, rest_ref)], axis=1
+                ).reshape(width, span)
                 acc[e] = acc[e] + jnp.dot(x, w, preferred_element_type=F32)
         for e in range(per_device):
             pre = acc[e] * (d_model ** (-0.5))
@@ -162,7 +168,7 @@
     me = jnp.stack([lax.axis_index("tp_0"), lax.axis_index("tp_1")]).astype(jnp.int32)
     return pl.pallas_call(
         kernel,
-        in_specs=[pl.BlockSpec(memory_space=pltpu.SMEM), vmem]
+        in_specs=[pl.BlockSpec(memory_space=pltpu.SMEM), vmem, vmem]
         + [pl.BlockSpec(memory_space=pltpu.HBM)] * len(pieces),
         out_specs=vmem,
         scratch_shapes=[
@@ -172,7 +178,51 @@
         out_shape=jax.ShapeDtypeStruct((per_device * slots, unit), BF16),
         compiler_params=pltpu.CompilerParams(vmem_limit_bytes=8 * MIB),
         name="hidden_units",
-    )(me, both, *(pltpu.with_memory_space_constraint(p, pltpu.HBM) for p in pieces))
+    )(me, top, rest, *(pltpu.with_memory_space_constraint(p, pltpu.HBM) for p in pieces))
+
+
+def ahead_along_z(blocks, nz, nx):
+    z = lax.axis_index("fs") // nx
+    by_z = blocks.reshape(nz, nx, *blocks.shape[1:])
+    result = []
+    for d in range(nz):
+        sent = lax.dynamic_index_in_dim(by_z, (z + d) % nz, 0, keepdims=False)
+        pairs = [(a * nx + b, ((a + d) % nz) * nx + b) for a in range(nz) for b in range(nx)]
+        result.append(sent if d == 0 else lax.ppermute(sent, "fs", pairs))
+    return result
+
+
+def then_along_x(pieces, nz, nx):
+    x = lax.axis_index("fs") % nx
+    result = []
+    for d in range(nx):
+        sent = jnp.stack(
+            [lax.dynamic_index_in_dim(p, (x + d) % nx, 0, keepdims=False) for p in pieces]
+        )
+        pairs = [(a * nx + b, a * nx + (b + d) % nx) for a in range(nz) for b in range(nx)]
+        result.append(sent if d == 0 else lax.ppermute(sent, "fs", pairs))
+    return result
+
+
+def sources_in_order(pieces, nz, nx):
+    block = pieces[0].shape[1:]
+
+    def kernel(me_ref, *refs):
+        z, x = me_ref[0] // nx, me_ref[0] % nx
+        for dx, ref in enumerate(refs[:-1]):
+            for dz in range(nz):
+                source = lax.rem(z - dz + nz, nz) * nx + lax.rem(x - dx + nx, nx)
+                refs[-1][pl.ds(source, 1)] = ref[dz : dz + 1]
+
+    vmem = pl.BlockSpec(memory_space=pltpu.VMEM)
+    return pl.pallas_call(
+        kernel,
+        in_specs=[pl.BlockSpec(memory_space=pltpu.SMEM)] + [vmem] * nx,
+        out_specs=vmem,
+        out_shape=jax.ShapeDtypeStruct((nz * nx, *block), BF16),
+        compiler_params=pltpu.CompilerParams(vmem_limit_bytes=8 * MIB),
+        name="sources_in_order",
+    )(lax.axis_index("fs").astype(jnp.int32).reshape(1), *pieces)
 
 
 def down_projected(hidden, down, per_device, capacity, scale):
@@ -205,7 +255,7 @@
 
 def work(tokens, route_ids, route_weights, norm_gain, gate_weight, up_weight, down_weight):
     tok_rows, d_model = tokens.shape
-    experts, _, hidden_local = gate_weight.shape
+    experts, rows_here, hidden_local = gate_weight.shape
     sources = lax.axis_size("fs")
     n_tp = lax.axis_size(TP)
     per_device = experts // sources
@@ -225,14 +275,19 @@
         ],
         axis=2,
     )
-    folded, first = lax.optimization_barrier((folded, first))
+    nz, nx = FS_SHAPE
+    ahead = rows_here // 4
+    early = ahead_along_z(folded[:, :ahead], nz, nx)
+    later, first = lax.optimization_barrier((folded[:, ahead:], first))
     arrived = first[:, :slots_out]
     down_both = first[:, slots_out:].reshape(d_model, per_device * hidden_local)
-    both = exchange(folded, "fs").reshape(d_model, 2 * per_device * hidden_local)
+    rest = exchange(later, "fs")
+    early = then_along_x(early, nz, nx)
+    top = sources_in_order(early, nz, nx)
 
     down_tp = spread_over_tp(down_both.reshape(n_tp, col_width, per_device * hidden_local))
     pieces = gathered_over_tp(arrived)
-    hidden = hidden_units(pieces, both, per_device, capacity)
+    hidden = hidden_units(pieces, top, rest, per_device, capacity)
     whole = gathered_over_tp(hidden)
     back = down_projected(whole, down_tp, per_device, capacity, (hidden_local * n_tp) ** (-0.5))
     back = exchange(back, "fs")
@@ -240,11 +295,13 @@
     combined = lax.dot_general(
         weight, back, (((0,), (0,)), ((), ())), precision=lax.Precision.HIGHEST
     )
+    both = jnp.concatenate([top, rest], axis=1).reshape(d_model, 2 * per_device * hidden_local)
     parts = [both[:, i * hidden_local : (i + 1) * hidden_local] for i in range(2 * per_device)]
+    gate_served, up_served = jnp.stack(parts[0::2]), jnp.stack(parts[1::2])
     down_served = jnp.stack(
         [down_both[:, e * hidden_local : (e + 1) * hidden_local] for e in range(per_device)]
     )
-    return (jnp.stack(parts[0::2]), jnp.stack(parts[1::2]), down_served, combined.astype(BF16))
+    return (gate_served, up_served, down_served, combined.astype(BF16))
 
 
 def solution(mesh):

time: 141 us -> 181 us (1.28)
  starting transfers between devices: 41.6 us -> 66.3 us
  local copies, waits for them, and re-layouts: 2.19 us -> 12.8 us
  other arithmetic: 6.47 us -> 11.7 us
    ppermute x0 -> x10, waiting for transfers between devices: none -> 35 us  [the longest x7 30.3 us: ahead_along_z(): result.append(sent if d == 0 else lax.ppermute(sent, 'fs', pairs))]
    all_to_all x3, waiting for transfers between devices: 64 us -> 37.3 us  [exchange(): return lax.all_to_all(blocks, axis, split_axis=0, concat_axis=0, tiled=True)]
    ppermute x0 -> x10, starting transfers between devices: none -> 20.3 us  [the longest x7 16.8 us: ahead_along_z(): result.append(sent if d == 0 else lax.ppermute(sent, 'fs', pairs))]
    ppermute x21, waiting for transfers between devices: 16.9 us -> 7.9 us  [moved(): return lax.ppermute(x, TP, pairs)]
    unnamed x14 -> x29, local copies, waits for them, and re-layouts: 0.03 us -> 7.28 us
    all_to_all x3, starting transfers between devices: 24.5 us -> 29.5 us  [exchange(): return lax.all_to_all(blocks, axis, split_axis=0, concat_axis=0, tiled=True)]
  transfers between devices with their start and end apart: 24 -> 34, of which waited for: 10 -> 14; matrix products, arithmetic and copies ran while one was open for 6% -> 12% of each run, Pallas kernels for 2% -> 1%
where the time goes in v1:
time: 181 us; the launch traced here: 180 us
  waiting for transfers between devices  80.2 us (44%)
  starting transfers between devices  66.3 us (37%)
  local copies, waits for them, and re-layouts  12.8 us (7%)
  other arithmetic  11.7 us (6%)
  Pallas kernels  7.1 us (4%)
    all_to_all x3, waiting for transfers between devices, exchange(): return lax.all_to_all(blocks, axis, split_axis=0, concat_axis=0, tiled=True)  37.3 us
    ppermute x7, waiting for transfers between devices, ahead_along_z(): result.append(sent if d == 0 else lax.ppermute(sent, 'fs', pairs))  30.3 us
    all_to_all x3, starting transfers between devices, exchange(): return lax.all_to_all(blocks, axis, split_axis=0, concat_axis=0, tiled=True)  29.5 us
    ppermute x7, starting transfers between devices, ahead_along_z(): result.append(sent if d == 0 else lax.ppermute(sent, 'fs', pairs))  16.8 us
    ppermute x21, starting transfers between devices, moved(): return lax.ppermute(x, TP, pairs)  16.6 us
    ppermute x21, waiting for transfers between devices, moved(): return lax.ppermute(x, TP, pairs)  7.9 us
    unnamed x29, local copies, waits for them, and re-layouts  7.28 us
    ppermute x3, waiting for transfers between devices, then_along_x(): result.append(sent if d == 0 else lax.ppermute(sent, 'fs', pairs))  4.75 us
  transfers between devices with their start and end apart: 34, of which 14 were waited for; matrix products, arithmetic and copies ran while one was open for 12% of the time, Pallas kernels for 1%

profile of v1, /device:TPU:32, one launch (start us, length us, event | category | flops | bytes accessed | tf_op | source)
XLA Modules:
  0.0 180.1 jit_solution(18134920175008721783)
XLA Ops:
  0.6 3.2 %prelude.1 = (bf16[32,80,256]{2,1,0:T(8,128)(2,1)}, f32[512,128]{1,0:T(8,128)}) custom-call(s32[1]{0:T(128)} %bitcast.13.me_ref, bf16[128,2048]{1,0:T(8,128)(2,1)} %own_ref.1, bf16[128,2048]{1,0:T(8,128)(2,1)} %own_ref.1, s32[2,128]{1,0:T(2,128)} %bitcast.69, f32[2,128]{1,0:T(2,128)} %bitcast.70, f32[64,64,128]{2,1,0:T(8,128)} %down_ref.1), custom_call_target="tpu_custom_call" | custom-call | tf_op jit(solution)/shard_map/prelude/pallas_call | solution.py:110
  3.8 11.3 %all-to-all-start = ((bf16[32,80,256]{2,1,0:T(8,128)(2,1)}), bf16[32,80,256]{2,1,0:T(8,128)(2,1)S(1)}, u32[]{:S(2)}, u32[]{:S(2)}) async-start(bf16[32,80,256]{2,1,0:T(8,128)(2,1)} %get-tuple-element.8), calls=%async_computation | async-start | bytes 2621440 | tf_op jit(solution)/shard_map/all_to_all | solution.py:19
  15.2 3.8 %multiply_convert_fusion.3 = (bf16[32,64,128]{2,1,0:T(8,128)(2,1)S(1)}, bf16[32,64,128]{2,1,0:T(8,128)(2,1)}, bf16[32,64,128]{2,1,0:T(8,128)(2,1)}, bf16[32,64,128]{2,1,0:T(8,128)(2,1)}) fusion(f32[64,64,128]{2,1,0:T(8,128)} %param.11, f32[64]{0:T(128)S(1)} %copy-done.10, f32[64,64,128]{2,1,0:T(8,128)} %param.12), kind=kLoop, calls=%fused_computation.11 | loop fusion | flops 2097152 | bytes 6291712 | tf_op jit(solution)/shard_map/convert_element_type | solution.py:272
  19.0 2.6 %pad_maximum_fusion.1 = bf16[32,48,512]{2,1,0:T(8,128)(2,1)} fusion(bf16[32,64,128]{2,1,0:T(8,128)(2,1)} %get-tuple-element.69, bf16[32,64,128]{2,1,0:T(8,128)(2,1)} %get-tuple-element.13, bf16[32,64,128]{2,1,0:T(8,128)(2,1)} %get-tuple-element.70, bf16[32,64,128]{2,1,0:T(8,128)(2,1)S(1)} %get-tuple-element.12), kind=kLoop, calls=%fused_computation.1 | loop fusion | flops 6291456 | bytes 3670016 | tf_op jit(solution)/shard_map/concatenate | solution.py:270
  21.6 26.4 %all-to-all-done = bf16[32,80,256]{2,1,0:T(8,128)(2,1)S(1)} async-done(((bf16[32,80,256]{2,1,0:T(8,128)(2,1)}), bf16[32,80,256]{2,1,0:T(8,128)(2,1)S(1)}, u32[]{:S(2)}, u32[]{:S(2)}) %all-to-all-start) | async-done | bytes 1310752 | tf_op jit(solution)/shard_map/all_to_all | solution.py:19
  48.0 6.5 %all-to-all-start.1 = ((bf16[32,48,512]{2,1,0:T(8,128)(2,1)}), bf16[32,48,512]{2,1,0:T(8,128)(2,1)S(1)}, u32[]{:S(2)}, u32[]{:S(2)}) async-start(bf16[32,48,512]{2,1,0:T(8,128)(2,1)} %pad_maximum_fusion.1), calls=%async_computation.1 | async-start | bytes 3145728 | tf_op jit(solution)/shard_map/all_to_all | solution.py:19
  54.6 1.1 pad_maximum_fusion.7
  55.7 0.8 copy-done.2
  56.5 0.7 dynamic-slice_bitcast_fusion.8
  57.4 3.9 %collective-permute-start.5 = (bf16[4,16,512]{2,1,0:T(8,128)(2,1)S(1)}, bf16[4,16,512]{2,1,0:T(8,128)(2,1)S(1)}, u32[]{:S(2)}, u32[]{:S(2)}) collective-permute-start(bf16[4,16,512]{2,1,0:T(8,128)(2,1)S(1)} %get-tuple-element.35), channel_id=1, source_target_pairs={{0,192},{8,200},{16,208},{24,216},{32,224},{40,232},{48,240},{56,2... | collective-permute-start | bytes 196616 | tf_op jit(solution)/shard_map/ppermute | solution.py:191
  61.4 2.3 %collective-permute-start.4 = (bf16[4,16,512]{2,1,0:T(8,128)(2,1)}, bf16[4,16,512]{2,1,0:T(8,128)(2,1)S(1)}, u32[]{:S(2)}, u32[]{:S(2)}) collective-permute-start(bf16[4,16,512]{2,1,0:T(8,128)(2,1)} %get-tuple-element.36), channel_id=1, source_target_pairs={{0,160},{8,168},{16,176},{24,184},{32,192},{40,200},{48,208},{56,2... | collective-permute-start | bytes 196616 | tf_op jit(solution)/shard_map/ppermute | solution.py:191
  63.7 2.7 %collective-permute-start.3 = (bf16[4,16,512]{2,1,0:T(8,128)(2,1)}, bf16[4,16,512]{2,1,0:T(8,128)(2,1)S(1)}, u32[]{:S(2)}, u32[]{:S(2)}) collective-permute-start(bf16[4,16,512]{2,1,0:T(8,128)(2,1)} %get-tuple-element.37), channel_id=1, source_target_pairs={{0,128},{8,136},{16,144},{24,152},{32,160},{40,168},{48,176},{56,1... | collective-permute-start | bytes 196616 | tf_op jit(solution)/shard_map/ppermute | solution.py:191
  66.4 1.4 constant_dynamic-update-slice_fusion.31
  67.8 22.9 %collective-permute-done = bf16[4,16,512]{2,1,0:T(8,128)(2,1)S(1)} collective-permute-done((bf16[4,16,512]{2,1,0:T(8,128)(2,1)S(1)}, bf16[4,16,512]{2,1,0:T(8,128)(2,1)S(1)}, u32[]{:S(2)}, u32[]{:S(2)}) %collective-permute-start) | collective-permute-done | bytes 65568 | tf_op jit(solution)/shard_map/ppermute | solution.py:191
  90.7 3.7 %collective-permute-start.1 = (bf16[4,16,512]{2,1,0:T(8,128)(2,1)}, bf16[4,16,512]{2,1,0:T(8,128)(2,1)S(1)}, u32[]{:S(2)}, u32[]{:S(2)}) collective-permute-start(bf16[4,16,512]{2,1,0:T(8,128)(2,1)} %get-tuple-element.39), channel_id=1, source_target_pairs={{0,64},{8,72},{16,80},{24,88},{32,96},{40,104},{48,112},{56,120},{... | collective-permute-start | bytes 196616 | tf_op jit(solution)/shard_map/ppermute | solution.py:191
  95.0 4.3 %collective-permute-done.1 = bf16[4,16,512]{2,1,0:T(8,128)(2,1)S(1)} collective-permute-done((bf16[4,16,512]{2,1,0:T(8,128)(2,1)}, bf16[4,16,512]{2,1,0:T(8,128)(2,1)S(1)}, u32[]{:S(2)}, u32[]{:S(2)}) %collective-permute-start.1) | collective-permute-done | bytes 65568 | tf_op jit(solution)/shard_map/ppermute | solution.py:191
  99.3 3.8 %collective-permute-start.2 = (bf16[4,16,512]{2,1,0:T(8,128)(2,1)}, bf16[4,16,512]{2,1,0:T(8,128)(2,1)S(1)}, u32[]{:S(2)}, u32[]{:S(2)}) collective-permute-start(bf16[4,16,512]{2,1,0:T(8,128)(2,1)} %get-tuple-element.38), channel_id=1, source_target_pairs={{0,96},{8,104},{16,112},{24,120},{32,128},{40,136},{48,144},{56,15... | collective-permute-start | bytes 196616 | tf_op jit(solution)/shard_map/ppermute | solution.py:191
  103.8 3.1 %collective-permute-done.2 = bf16[4,16,512]{2,1,0:T(8,128)(2,1)S(1)} collective-permute-done((bf16[4,16,512]{2,1,0:T(8,128)(2,1)}, bf16[4,16,512]{2,1,0:T(8,128)(2,1)S(1)}, u32[]{:S(2)}, u32[]{:S(2)}) %collective-permute-start.2) | collective-permute-done | bytes 65568 | tf_op jit(solution)/shard_map/ppermute | solution.py:191
  108.7 0.7 slice.55.refs_0_
  109.4 3.0 %collective-permute-start.15 = (bf16[32,16,256]{2,1,0:T(8,128)(2,1)}, bf16[32,16,256]{2,1,0:T(8,128)(2,1)}, u32[]{:S(2)}, u32[]{:S(2)}) collective-permute-start(bf16[32,16,256]{2,1,0:T(8,128)(2,1)} %slice.55.refs_0_), channel_id=1, source_target_pairs={{0,6},{1,7},{2,0},{3,1},{4,2},{5,3},{6,4},{7,5},{8,14},{9,15},{10,... | collective-permute-start | bytes 786440 | tf_op jit(solution)/shard_map/ppermute | solution.py:29
  114.3 2.0 %collective-permute-start.9 = (bf16[8,16,512]{2,1,0:T(8,128)(2,1)S(1)}, bf16[8,16,512]{2,1,0:T(8,128)(2,1)S(1)}, u32[]{:S(2)}, u32[]{:S(2)}) collective-permute-start(bf16[8,16,512]{2,1,0:T(8,128)(2,1)S(1)} %get-tuple-element.41), channel_id=1, source_target_pairs={{0,24},{8,0},{16,8},{24,16},{32,56},{40,32},{48,40},{56,48},{64,88... | collective-permute-start | bytes 393224 | tf_op jit(solution)/shard_map/ppermute | solution.py:203
  116.3 0.8 collective-permute-start.8
  117.8 2.5 %collective-permute-done.9.refs_3_ = bf16[8,16,512]{2,1,0:T(8,128)(2,1)S(1)} collective-permute-done((bf16[8,16,512]{2,1,0:T(8,128)(2,1)S(1)}, bf16[8,16,512]{2,1,0:T(8,128)(2,1)S(1)}, u32[]{:S(2)}, u32[]{:S(2)}) %collective-permute-start.9) | collective-permute-done | bytes 131104 | tf_op jit(solution)/shard_map/ppermute | solution.py:203
  120.3 1.0 collective-permute-start.11
  121.2 1.6 collective-permute-done.8.refs_2_
  124.3 1.3 slice.52
  125.6 0.9 dynamic-slice_bitcast_fusion
  127.1 1.1 collective-permute-done.11.refs_2_
  128.2 1.2 collective-permute-start.29
  129.4 0.7 collective-permute-start.28
  130.1 3.0 %collective-permute-start.27 = (bf16[256,256]{1,0:T(8,128)(2,1)}, bf16[256,256]{1,0:T(8,128)(2,1)S(1)}, u32[]{:S(2)}, u32[]{:S(2)}) collective-permute-start(bf16[256,256]{1,0:T(8,128)(2,1)} %get-tuple-element.23), channel_id=1, source_target_pairs={{0,4},{1,5},{2,6},{3,7},{4,0},{5,1},{6,2},{7,3},{8,12},{9,13},{10,... | collective-permute-start | bytes 393224 | tf_op jit(solution)/shard_map/ppermute | solution.py:29
  133.1 0.7 copy-done.6
  133.8 0.9 slice_bitcast_fusion.1
  134.8 0.7 copy-done.7
  135.7 2.6 %hidden_units.1.refs_0_ = bf16[512,128]{1,0:T(8,128)(2,1)S(1)} custom-call(s32[2]{0:T(128)S(1)} %pad_add_fusion.me_ref, bf16[32,16,512]{2,1,0:T(8,128)(2,1)S(1)} %sources_in_order.1.top_ref, bf16[32,48,512]{2,1,0:T(8,128)(2,1)S(1)} %all-to-all-done.1.rest_ref, bf16[32,16,256]{2,1,0:T(8,128)(2,1)} %slice.55.refs_0_, bf16[32,16,256]{2,1,0:T(8,128)(2,1)} %copy-done.4, ...), custom_call_target="tpu_custom_call" | custom-call | tf_op jit(solution)/shard_map/hidden_units/pallas_call | solution.py:169
  138.6 3.1 %collective-permute-start.22 = (bf16[512,128]{1,0:T(8,128)(2,1)S(1)}, bf16[512,128]{1,0:T(8,128)(2,1)S(1)}, u32[]{:S(2)}, u32[]{:S(2)}) collective-permute-start(bf16[512,128]{1,0:T(8,128)(2,1)S(1)} %hidden_units.1.refs_0_), channel_id=1, source_target_pairs={{0,6},{1,7},{2,0},{3,1},{4,2},{5,3},{6,4},{7,5},{8,14},{9,15},{10,... | collective-permute-start | bytes 393224 | tf_op jit(solution)/shard_map/ppermute | solution.py:29
  141.7 1.1 collective-permute-start.20
  142.8 1.3 collective-permute-start.18
  144.2 1.1 pad_maximum_fusion.6
  145.8 1.8 collective-permute-done.22.refs_6_
  147.5 2.4 %collective-permute-done.20.refs_4_ = bf16[512,128]{1,0:T(8,128)(2,1)S(1)} collective-permute-done((bf16[512,128]{1,0:T(8,128)(2,1)S(1)}, bf16[512,128]{1,0:T(8,128)(2,1)S(1)}, u32[]{:S(2)}, u32[]{:S(2)}) %collective-permute-start.20) | collective-permute-done | bytes 131104 | tf_op jit(solution)/shard_map/ppermute | solution.py:29
  149.9 1.9 %collective-permute-done.18.refs_2_ = bf16[512,128]{1,0:T(8,128)(2,1)S(1)} collective-permute-done((bf16[512,128]{1,0:T(8,128)(2,1)S(1)}, bf16[512,128]{1,0:T(8,128)(2,1)S(1)}, u32[]{:S(2)}, u32[]{:S(2)}) %collective-permute-start.18) | collective-permute-done | bytes 131104 | tf_op jit(solution)/shard_map/ppermute | solution.py:29
  151.8 1.6 pad_maximum_fusion
  153.4 1.2 down_projected.1
  154.6 11.7 %all-to-all-start.2 = ((bf16[32,16,256]{2,1,0:T(8,128)(2,1)}), bf16[32,16,256]{2,1,0:T(8,128)(2,1)S(1)}, u32[]{:S(2)}, u32[]{:S(2)}) async-start(bf16[32,16,256]{2,1,0:T(8,128)(2,1)} %down_projected.1), calls=%async_computation.2 | async-start | bytes 524288 | tf_op jit(solution)/shard_map/all_to_all | solution.py:19
  166.7 1.5 pad_maximum_fusion.4
  168.2 10.9 %all-to-all-done.2 = bf16[32,16,256]{2,1,0:T(8,128)(2,1)S(1)} async-done(((bf16[32,16,256]{2,1,0:T(8,128)(2,1)}), bf16[32,16,256]{2,1,0:T(8,128)(2,1)S(1)}, u32[]{:S(2)}, u32[]{:S(2)}) %all-to-all-start.2) | async-done | bytes 262176 | tf_op jit(solution)/shard_map/all_to_all | solution.py:19
  179.1 1.0 convolution_convert_fusion
  (68 shorter events, 9.3 us)
Async XLA Ops:
  3.8 11.3 %copy-start.10 = (f32[64]{0:T(128)S(1)}, f32[64]{0:T(128)}, u32[]{:S(2)}) copy-start(f32[64]{0:T(128)} %param.10) | copy-start | bytes 772
  3.8 44.1 %all-to-all-start = ((bf16[32,80,256]{2,1,0:T(8,128)(2,1)}), bf16[32,80,256]{2,1,0:T(8,128)(2,1)S(1)}, u32[]{:S(2)}, u32[]{:S(2)}) async-start(bf16[32,80,256]{2,1,0:T(8,128)(2,1)} %get-tuple-element.8), calls=%async_computation | async-start | bytes 2621440 | tf_op jit(solution)/shard_map/all_to_all | solution.py:19
  48.0 66.3 %copy-start.1 = (bf16[32,80,256]{2,1,0:T(8,128)(2,1)}, bf16[32,80,256]{2,1,0:T(8,128)(2,1)S(1)}, u32[]{:S(2)}) copy-start(bf16[32,80,256]{2,1,0:T(8,128)(2,1)S(1)} %all-to-all-done) | copy-start | bytes 3932164
  48.0 87.7 %all-to-all-start.1 = ((bf16[32,48,512]{2,1,0:T(8,128)(2,1)}), bf16[32,48,512]{2,1,0:T(8,128)(2,1)S(1)}, u32[]{:S(2)}, u32[]{:S(2)}) async-start(bf16[32,48,512]{2,1,0:T(8,128)(2,1)} %pad_maximum_fusion.1), calls=%async_computation.1 | async-start | bytes 3145728 | tf_op jit(solution)/shard_map/all_to_all | solution.py:19
  55.7 0.8 copy-start.2
  57.2 56.5 %collective-permute-start.6 = (bf16[4,16,512]{2,1,0:T(8,128)(2,1)S(1)}, bf16[4,16,512]{2,1,0:T(8,128)(2,1)S(1)}, u32[]{:S(2)}, u32[]{:S(2)}) collective-permute-start(bf16[4,16,512]{2,1,0:T(8,128)(2,1)S(1)} %get-tuple-element.34), channel_id=1, source_target_pairs={{0,224},{8,232},{16,240},{24,248},{32,0},{40,8},{48,16},{56,24},{6... | collective-permute-start | bytes 196616 | tf_op jit(solution)/shard_map/ppermute | solution.py:191
  57.4 55.6 %collective-permute-start.5 = (bf16[4,16,512]{2,1,0:T(8,128)(2,1)S(1)}, bf16[4,16,512]{2,1,0:T(8,128)(2,1)S(1)}, u32[]{:S(2)}, u32[]{:S(2)}) collective-permute-start(bf16[4,16,512]{2,1,0:T(8,128)(2,1)S(1)} %get-tuple-element.35), channel_id=1, source_target_pairs={{0,192},{8,200},{16,208},{24,216},{32,224},{40,232},{48,240},{56,2... | collective-permute-start | bytes 196616 | tf_op jit(solution)/shard_map/ppermute | solution.py:191
  61.4 46.7 %collective-permute-start.4 = (bf16[4,16,512]{2,1,0:T(8,128)(2,1)}, bf16[4,16,512]{2,1,0:T(8,128)(2,1)S(1)}, u32[]{:S(2)}, u32[]{:S(2)}) collective-permute-start(bf16[4,16,512]{2,1,0:T(8,128)(2,1)} %get-tuple-element.36), channel_id=1, source_target_pairs={{0,160},{8,168},{16,176},{24,184},{32,192},{40,200},{48,208},{56,2... | collective-permute-start | bytes 196616 | tf_op jit(solution)/shard_map/ppermute | solution.py:191
  63.7 43.8 %collective-permute-start.3 = (bf16[4,16,512]{2,1,0:T(8,128)(2,1)}, bf16[4,16,512]{2,1,0:T(8,128)(2,1)S(1)}, u32[]{:S(2)}, u32[]{:S(2)}) collective-permute-start(bf16[4,16,512]{2,1,0:T(8,128)(2,1)} %get-tuple-element.37), channel_id=1, source_target_pairs={{0,128},{8,136},{16,144},{24,152},{32,160},{40,168},{48,176},{56,1... | collective-permute-start | bytes 196616 | tf_op jit(solution)/shard_map/ppermute | solution.py:191
  66.4 24.3 %collective-permute-start = (bf16[4,16,512]{2,1,0:T(8,128)(2,1)S(1)}, bf16[4,16,512]{2,1,0:T(8,128)(2,1)S(1)}, u32[]{:S(2)}, u32[]{:S(2)}) collective-permute-start(bf16[4,16,512]{2,1,0:T(8,128)(2,1)S(1)} %get-tuple-element.40), channel_id=1, source_target_pairs={{0,32},{8,40},{16,48},{24,56},{32,64},{40,72},{48,80},{56,88},{64,... | collective-permute-start | bytes 196616 | tf_op jit(solution)/shard_map/ppermute | solution.py:191
  90.7 8.6 %collective-permute-start.1 = (bf16[4,16,512]{2,1,0:T(8,128)(2,1)}, bf16[4,16,512]{2,1,0:T(8,128)(2,1)S(1)}, u32[]{:S(2)}, u32[]{:S(2)}) collective-permute-start(bf16[4,16,512]{2,1,0:T(8,128)(2,1)} %get-tuple-element.39), channel_id=1, source_target_pairs={{0,64},{8,72},{16,80},{24,88},{32,96},{40,104},{48,112},{56,120},{... | collective-permute-start | bytes 196616 | tf_op jit(solution)/shard_map/ppermute | solution.py:191
  99.3 7.6 %collective-permute-start.2 = (bf16[4,16,512]{2,1,0:T(8,128)(2,1)}, bf16[4,16,512]{2,1,0:T(8,128)(2,1)S(1)}, u32[]{:S(2)}, u32[]{:S(2)}) collective-permute-start(bf16[4,16,512]{2,1,0:T(8,128)(2,1)} %get-tuple-element.38), channel_id=1, source_target_pairs={{0,96},{8,104},{16,112},{24,120},{32,128},{40,136},{48,144},{56,15... | collective-permute-start | bytes 196616 | tf_op jit(solution)/shard_map/ppermute | solution.py:191
  109.4 13.4 %collective-permute-start.15 = (bf16[32,16,256]{2,1,0:T(8,128)(2,1)}, bf16[32,16,256]{2,1,0:T(8,128)(2,1)}, u32[]{:S(2)}, u32[]{:S(2)}) collective-permute-start(bf16[32,16,256]{2,1,0:T(8,128)(2,1)} %slice.55.refs_0_), channel_id=1, source_target_pairs={{0,6},{1,7},{2,0},{3,1},{4,2},{5,3},{6,4},{7,5},{8,14},{9,15},{10,... | collective-permute-start | bytes 786440 | tf_op jit(solution)/shard_map/ppermute | solution.py:29
  112.4 10.9 %collective-permute-start.13 = (bf16[32,16,256]{2,1,0:T(8,128)(2,1)}, bf16[32,16,256]{2,1,0:T(8,128)(2,1)}, u32[]{:S(2)}, u32[]{:S(2)}) collective-permute-start(bf16[32,16,256]{2,1,0:T(8,128)(2,1)} %slice.55.refs_0_), channel_id=1, source_target_pairs={{0,4},{1,5},{2,6},{3,7},{4,0},{5,1},{6,2},{7,3},{8,12},{9,13},{10,... | collective-permute-start | bytes 786440 | tf_op jit(solution)/shard_map/ppermute | solution.py:29
  114.3 6.0 %collective-permute-start.9 = (bf16[8,16,512]{2,1,0:T(8,128)(2,1)S(1)}, bf16[8,16,512]{2,1,0:T(8,128)(2,1)S(1)}, u32[]{:S(2)}, u32[]{:S(2)}) collective-permute-start(bf16[8,16,512]{2,1,0:T(8,128)(2,1)S(1)} %get-tuple-element.41), channel_id=1, source_target_pairs={{0,24},{8,0},{16,8},{24,16},{32,56},{40,32},{48,40},{56,48},{64,88... | collective-permute-start | bytes 393224 | tf_op jit(solution)/shard_map/ppermute | solution.py:203
  116.3 6.5 %collective-permute-start.8 = (bf16[8,16,512]{2,1,0:T(8,128)(2,1)S(1)}, bf16[8,16,512]{2,1,0:T(8,128)(2,1)S(1)}, u32[]{:S(2)}, u32[]{:S(2)}) collective-permute-start(bf16[8,16,512]{2,1,0:T(8,128)(2,1)S(1)} %get-tuple-element.42), channel_id=1, source_target_pairs={{0,16},{8,24},{16,0},{24,8},{32,48},{40,56},{48,32},{56,40},{64,80... | collective-permute-start | bytes 393224 | tf_op jit(solution)/shard_map/ppermute | solution.py:203
  117.2 7.0 %collective-permute-start.7 = (bf16[8,16,512]{2,1,0:T(8,128)(2,1)}, bf16[8,16,512]{2,1,0:T(8,128)(2,1)S(1)}, u32[]{:S(2)}, u32[]{:S(2)}) collective-permute-start(bf16[8,16,512]{2,1,0:T(8,128)(2,1)} %get-tuple-element.43), channel_id=1, source_target_pairs={{0,8},{8,16},{16,24},{24,0},{32,40},{40,48},{48,56},{56,32},{64,72... | collective-permute-start | bytes 393224 | tf_op jit(solution)/shard_map/ppermute | solution.py:203
  120.3 7.9 %collective-permute-start.11 = (bf16[32,16,256]{2,1,0:T(8,128)(2,1)}, bf16[32,16,256]{2,1,0:T(8,128)(2,1)}, u32[]{:S(2)}, u32[]{:S(2)}) collective-permute-start(bf16[32,16,256]{2,1,0:T(8,128)(2,1)} %slice.55.refs_0_), channel_id=1, source_target_pairs={{0,2},{1,3},{2,4},{3,5},{4,6},{5,7},{6,0},{7,1},{8,10},{9,11},{10,... | collective-permute-start | bytes 786440 | tf_op jit(solution)/shard_map/ppermute | solution.py:29
  122.9 6.5 %collective-permute-start.10 = (bf16[32,16,256]{2,1,0:T(8,128)(2,1)}, bf16[32,16,256]{2,1,0:T(8,128)(2,1)S(1)}, u32[]{:S(2)}, u32[]{:S(2)}) collective-permute-start(bf16[32,16,256]{2,1,0:T(8,128)(2,1)} %slice.55.refs_0_), channel_id=1, source_target_pairs={{0,1},{1,0},{2,3},{3,2},{4,5},{5,4},{6,7},{7,6},{8,9},{9,8},{10,11... | collective-permute-start | bytes 786440 | tf_op jit(solution)/shard_map/ppermute | solution.py:29
  122.9 7.2 %collective-permute-start.16 = (bf16[32,16,256]{2,1,0:T(8,128)(2,1)}, bf16[32,16,256]{2,1,0:T(8,128)(2,1)S(1)}, u32[]{:S(2)}, u32[]{:S(2)}) collective-permute-start(bf16[32,16,256]{2,1,0:T(8,128)(2,1)} %collective-permute-done.15.refs_6_), channel_id=1, source_target_pairs={{0,1},{1,0},{2,3},{3,2},{4,5},{5,4},{6,7},{7,6},{8,9},{9,8},{10,11... | collective-permute-start | bytes 786440 | tf_op jit(solution)/shard_map/ppermute | solution.py:29
  123.4 9.7 %collective-permute-start.14 = (bf16[32,16,256]{2,1,0:T(8,128)(2,1)}, bf16[32,16,256]{2,1,0:T(8,128)(2,1)S(1)}, u32[]{:S(2)}, u32[]{:S(2)}) collective-permute-start(bf16[32,16,256]{2,1,0:T(8,128)(2,1)} %collective-permute-done.13.refs_4_), channel_id=1, source_target_pairs={{0,1},{1,0},{2,3},{3,2},{4,5},{5,4},{6,7},{7,6},{8,9},{9,8},{10,11... | collective-permute-start | bytes 786440 | tf_op jit(solution)/shard_map/ppermute | solution.py:29
  126.5 11.9 %collective-permute-start.30 = (bf16[256,256]{1,0:T(8,128)(2,1)}, bf16[256,256]{1,0:T(8,128)(2,1)S(1)}, u32[]{:S(2)}, u32[]{:S(2)}) collective-permute-start(bf16[256,256]{1,0:T(8,128)(2,1)} %get-tuple-element.20), channel_id=1, source_target_pairs={{0,7},{1,6},{2,1},{3,0},{4,3},{5,2},{6,5},{7,4},{8,15},{9,14},{10,... | collective-permute-start | bytes 393224 | tf_op jit(solution)/shard_map/ppermute | solution.py:29
  128.2 10.5 %collective-permute-start.29 = (bf16[256,256]{1,0:T(8,128)(2,1)}, bf16[256,256]{1,0:T(8,128)(2,1)S(1)}, u32[]{:S(2)}, u32[]{:S(2)}) collective-permute-start(bf16[256,256]{1,0:T(8,128)(2,1)} %get-tuple-element.21), channel_id=1, source_target_pairs={{0,6},{1,7},{2,0},{3,1},{4,2},{5,3},{6,4},{7,5},{8,14},{9,15},{10,... | collective-permute-start | bytes 393224 | tf_op jit(solution)/shard_map/ppermute | solution.py:29
  129.4 0.7 copy-start.4
  129.4 12.3 %collective-permute-start.28 = (bf16[256,256]{1,0:T(8,128)(2,1)}, bf16[256,256]{1,0:T(8,128)(2,1)S(1)}, u32[]{:S(2)}, u32[]{:S(2)}) collective-permute-start(bf16[256,256]{1,0:T(8,128)(2,1)} %get-tuple-element.22), channel_id=1, source_target_pairs={{0,5},{1,4},{2,7},{3,6},{4,1},{5,0},{6,3},{7,2},{8,13},{9,12},{10,... | collective-permute-start | bytes 393224 | tf_op jit(solution)/shard_map/ppermute | solution.py:29
  130.1 3.0 %copy-start.5 = (bf16[32,16,256]{2,1,0:T(8,128)(2,1)}, bf16[32,16,256]{2,1,0:T(8,128)(2,1)S(1)}, u32[]{:S(2)}) copy-start(bf16[32,16,256]{2,1,0:T(8,128)(2,1)S(1)} %collective-permute-done.16.refs_7_) | copy-start | bytes 786436
  130.1 12.7 %collective-permute-start.27 = (bf16[256,256]{1,0:T(8,128)(2,1)}, bf16[256,256]{1,0:T(8,128)(2,1)S(1)}, u32[]{:S(2)}, u32[]{:S(2)}) collective-permute-start(bf16[256,256]{1,0:T(8,128)(2,1)} %get-tuple-element.23), channel_id=1, source_target_pairs={{0,4},{1,5},{2,6},{3,7},{4,0},{5,1},{6,2},{7,3},{8,12},{9,13},{10,... | collective-permute-start | bytes 393224 | tf_op jit(solution)/shard_map/ppermute | solution.py:29
  133.1 0.7 copy-start.6
  133.1 1.7 collective-permute-start.12
  134.8 0.7 copy-start.7
  135.5 9.7 %collective-permute-start.26 = (bf16[256,256]{1,0:T(8,128)(2,1)}, bf16[256,256]{1,0:T(8,128)(2,1)S(1)}, u32[]{:S(2)}, u32[]{:S(2)}) collective-permute-start(bf16[256,256]{1,0:T(8,128)(2,1)} %get-tuple-element.24), channel_id=1, source_target_pairs={{0,3},{1,2},{2,5},{3,4},{4,7},{5,6},{6,1},{7,0},{8,11},{9,10},{10,... | collective-permute-start | bytes 393224 | tf_op jit(solution)/shard_map/ppermute | solution.py:29
  135.7 2.7 %copy-start.9 = (bf16[256,256]{1,0:T(8,128)(2,1)S(1)}, bf16[256,256]{1,0:T(8,128)(2,1)}, u32[]{:S(2)}) copy-start(bf16[256,256]{1,0:T(8,128)(2,1)} %get-tuple-element.25) | copy-start | bytes 393220
  135.7 8.4 %copy-start.3 = (bf16[1,2048,128]{2,1,0:T(8,128)(2,1)S(1)}, bf16[1,2048,128]{2,1,0:T(8,128)(2,1)}, u32[]{:S(2)}) copy-start(bf16[1,2048,128]{2,1,0:T(8,128)(2,1)} %get-tuple-element.29) | copy-start | bytes 1572868
  138.4 7.4 %collective-permute-start.25 = (bf16[256,256]{1,0:T(8,128)(2,1)S(1)}, bf16[256,256]{1,0:T(8,128)(2,1)S(1)}, u32[]{:S(2)}, u32[]{:S(2)}) collective-permute-start(bf16[256,256]{1,0:T(8,128)(2,1)S(1)} %copy-done.9), channel_id=1, source_target_pairs={{0,2},{1,3},{2,4},{3,5},{4,6},{5,7},{6,0},{7,1},{8,10},{9,11},{10,... | collective-permute-start | bytes 393224 | tf_op jit(solution)/shard_map/ppermute | solution.py:29
  138.6 8.9 %collective-permute-start.22 = (bf16[512,128]{1,0:T(8,128)(2,1)S(1)}, bf16[512,128]{1,0:T(8,128)(2,1)S(1)}, u32[]{:S(2)}, u32[]{:S(2)}) collective-permute-start(bf16[512,128]{1,0:T(8,128)(2,1)S(1)} %hidden_units.1.refs_0_), channel_id=1, source_target_pairs={{0,6},{1,7},{2,0},{3,1},{4,2},{5,3},{6,4},{7,5},{8,14},{9,15},{10,... | collective-permute-start | bytes 393224 | tf_op jit(solution)/shard_map/ppermute | solution.py:29
  141.7 8.2 %collective-permute-start.20 = (bf16[512,128]{1,0:T(8,128)(2,1)S(1)}, bf16[512,128]{1,0:T(8,128)(2,1)S(1)}, u32[]{:S(2)}, u32[]{:S(2)}) collective-permute-start(bf16[512,128]{1,0:T(8,128)(2,1)S(1)} %hidden_units.1.refs_0_), channel_id=1, source_target_pairs={{0,4},{1,5},{2,6},{3,7},{4,0},{5,1},{6,2},{7,3},{8,12},{9,13},{10,... | collective-permute-start | bytes 393224 | tf_op jit(solution)/shard_map/ppermute | solution.py:29
  142.8 9.0 %collective-permute-start.18 = (bf16[512,128]{1,0:T(8,128)(2,1)S(1)}, bf16[512,128]{1,0:T(8,128)(2,1)S(1)}, u32[]{:S(2)}, u32[]{:S(2)}) collective-permute-start(bf16[512,128]{1,0:T(8,128)(2,1)S(1)} %hidden_units.1.refs_0_), channel_id=1, source_target_pairs={{0,2},{1,3},{2,4},{3,5},{4,6},{5,7},{6,0},{7,1},{8,10},{9,11},{10,... | collective-permute-start | bytes 393224 | tf_op jit(solution)/shard_map/ppermute | solution.py:29
  145.2 8.2 %collective-permute-start.24 = (bf16[256,256]{1,0:T(8,128)(2,1)S(1)}, bf16[256,256]{1,0:T(8,128)(2,1)S(1)}, u32[]{:S(2)}, u32[]{:S(2)}) collective-permute-start(bf16[256,256]{1,0:T(8,128)(2,1)S(1)} %get-tuple-element.26), channel_id=1, source_target_pairs={{0,1},{1,0},{2,3},{3,2},{4,5},{5,4},{6,7},{7,6},{8,9},{9,8},{10,11... | collective-permute-start | bytes 393224 | tf_op jit(solution)/shard_map/ppermute | solution.py:29
  145.8 7.6 %collective-permute-start.17 = (bf16[512,128]{1,0:T(8,128)(2,1)S(1)}, bf16[512,128]{1,0:T(8,128)(2,1)S(1)}, u32[]{:S(2)}, u32[]{:S(2)}) collective-permute-start(bf16[512,128]{1,0:T(8,128)(2,1)S(1)} %hidden_units.1.refs_0_), channel_id=1, source_target_pairs={{0,1},{1,0},{2,3},{3,2},{4,5},{5,4},{6,7},{7,6},{8,9},{9,8},{10,11... | collective-permute-start | bytes 393224 | tf_op jit(solution)/shard_map/ppermute | solution.py:29
  147.5 5.9 %collective-permute-start.23 = (bf16[512,128]{1,0:T(8,128)(2,1)S(1)}, bf16[512,128]{1,0:T(8,128)(2,1)S(1)}, u32[]{:S(2)}, u32[]{:S(2)}) collective-permute-start(bf16[512,128]{1,0:T(8,128)(2,1)S(1)} %collective-permute-done.22.refs_6_), channel_id=1, source_target_pairs={{0,1},{1,0},{2,3},{3,2},{4,5},{5,4},{6,7},{7,6},{8,9},{9,8},{10,11... | collective-permute-start | bytes 393224 | tf_op jit(solution)/shard_map/ppermute | solution.py:29
  149.9 3.5 %collective-permute-start.21 = (bf16[512,128]{1,0:T(8,128)(2,1)S(1)}, bf16[512,128]{1,0:T(8,128)(2,1)S(1)}, u32[]{:S(2)}, u32[]{:S(2)}) collective-permute-start(bf16[512,128]{1,0:T(8,128)(2,1)S(1)} %collective-permute-done.20.refs_4_), channel_id=1, source_target_pairs={{0,1},{1,0},{2,3},{3,2},{4,5},{5,4},{6,7},{7,6},{8,9},{9,8},{10,11... | collective-permute-start | bytes 393224 | tf_op jit(solution)/shard_map/ppermute | solution.py:29
  151.8 1.6 collective-permute-start.19
  153.4 12.9 %copy-start = (bf16[32,64,512]{2,1,0:T(8,128)(2,1)S(1)}, bf16[32,64,512]{2,1,0:T(8,128)(2,1)}, u32[]{:S(2)}) copy-start(bf16[32,64,512]{2,1,0:T(8,128)(2,1)} %pad_maximum_fusion) | copy-start | bytes 6291460
  154.6 24.5 %all-to-all-start.2 = ((bf16[32,16,256]{2,1,0:T(8,128)(2,1)}), bf16[32,16,256]{2,1,0:T(8,128)(2,1)S(1)}, u32[]{:S(2)}, u32[]{:S(2)}) async-start(bf16[32,16,256]{2,1,0:T(8,128)(2,1)} %down_projected.1), calls=%async_computation.2 | async-start | bytes 524288 | tf_op jit(solution)/shard_map/all_to_all | solution.py:19
  166.7 12.4 %copy-start.8 = (f32[512,128]{1,0:T(8,128)S(1)}, f32[512,128]{1,0:T(8,128)}, u32[]{:S(2)}) copy-start(f32[512,128]{1,0:T(8,128)} %get-tuple-element.11) | copy-start | bytes 786436

commit v2 on v1

--- a/solution.py
+++ b/solution.py
@@ -192,13 +192,31 @@
     return result
 
 
+def by_column(pieces, nx):
+    block = pieces[0].shape[1:]
+    nz = len(pieces)
+
+    def kernel(me_ref, *refs):
+        for d, out_ref in enumerate(refs[nz:]):
+            column = lax.rem(me_ref[0] + d, nx)
+            for dz, ref in enumerate(refs[:nz]):
+                out_ref[dz : dz + 1] = ref[pl.ds(column, 1)]
+
+    vmem = pl.BlockSpec(memory_space=pltpu.VMEM)
+    x = lax.axis_index("fs") % nx
+    return pl.pallas_call(
+        kernel,
+        in_specs=[pl.BlockSpec(memory_space=pltpu.SMEM)] + [vmem] * nz,
+        out_specs=[vmem] * nx,
+        out_shape=[jax.ShapeDtypeStruct((nz, *block), BF16)] * nx,
+        compiler_params=pltpu.CompilerParams(vmem_limit_bytes=8 * MIB),
+        name="by_column",
+    )(x.astype(jnp.int32).reshape(1), *pieces)
+
+
 def then_along_x(pieces, nz, nx):
-    x = lax.axis_index("fs") % nx
     result = []
-    for d in range(nx):
-        sent = jnp.stack(
-            [lax.dynamic_index_in_dim(p, (x + d) % nx, 0, keepdims=False) for p in pieces]
-        )
+    for d, sent in enumerate(pieces):
         pairs = [(a * nx + b, a * nx + (b + d) % nx) for a in range(nz) for b in range(nx)]
         result.append(sent if d == 0 else lax.ppermute(sent, "fs", pairs))
     return result
@@ -282,6 +300,7 @@
     arrived = first[:, :slots_out]
     down_both = first[:, slots_out:].reshape(d_model, per_device * hidden_local)
     rest = exchange(later, "fs")
+    early = by_column(early, nx)
     early = then_along_x(early, nz, nx)
     top = sources_in_order(early, nz, nx)
 

time: 181 us -> 172 us (0.950)
  local copies, waits for them, and re-layouts: 12.8 us -> 5.78 us
    unnamed x29 -> x22, local copies, waits for them, and re-layouts: 7.28 us -> 1.52 us
    ppermute x21, starting transfers between devices: 16.6 us -> 21.9 us  [moved(): return lax.ppermute(x, TP, pairs)]
    all_to_all x3, starting transfers between devices: 29.5 us -> 24.6 us  [exchange(): return lax.all_to_all(blocks, axis, split_axis=0, concat_axis=0, tiled=True)]
    ppermute x7, starting transfers between devices: 16.8 us -> 14 us  [ahead_along_z(): result.append(sent if d == 0 else lax.ppermute(sent, 'fs', pairs))]
    ppermute x3, waiting for transfers between devices: 4.75 us -> 2.13 us  [then_along_x(): result.append(sent if d == 0 else lax.ppermute(sent, 'fs', pairs))]
    ppermute x3, starting transfers between devices: 3.49 us -> 5.6 us  [then_along_x(): result.append(sent if d == 0 else lax.ppermute(sent, 'fs', pairs))]
  transfers between devices with their start and end apart: 34 -> 34, of which waited for: 14 -> 14; matrix products, arithmetic and copies ran while one was open for 12% -> 9% of each run, Pallas kernels for 1% -> 2%
where the time goes in v2:
time: 172 us; the launch traced here: 171 us
  waiting for transfers between devices  78.5 us (46%)
  starting transfers between devices  66.1 us (38%)
  other arithmetic  11.7 us (7%)
  Pallas kernels  7.16 us (4%)
  local copies, waits for them, and re-layouts  5.78 us (3%)
    all_to_all x3, waiting for transfers between devices, exchange(): return lax.all_to_all(blocks, axis, split_axis=0, concat_axis=0, tiled=True)  36.5 us
    ppermute x7, waiting for transfers between devices, ahead_along_z(): result.append(sent if d == 0 else lax.ppermute(sent, 'fs', pairs))  31.3 us
    all_to_all x3, starting transfers between devices, exchange(): return lax.all_to_all(blocks, axis, split_axis=0, concat_axis=0, tiled=True)  24.6 us
    ppermute x21, starting transfers between devices, moved(): return lax.ppermute(x, TP, pairs)  21.9 us
    ppermute x7, starting transfers between devices, ahead_along_z(): result.append(sent if d == 0 else lax.ppermute(sent, 'fs', pairs))  14 us
    ppermute x21, waiting for transfers between devices, moved(): return lax.ppermute(x, TP, pairs)  8.56 us
    ppermute x3, starting transfers between devices, then_along_x(): result.append(sent if d == 0 else lax.ppermute(sent, 'fs', pairs))  5.6 us
    convert_element_type x1, other arithmetic, work(): (scaling * w[e::per_device]).astype(BF16)  3.73 us
  transfers between devices with their start and end apart: 34, of which 14 were waited for; matrix products, arithmetic and copies ran while one was open for 9% of the time, Pallas kernels for 2%

profile of v2, /device:TPU:32, one launch (start us, length us, event | category | flops | bytes accessed | tf_op | source)
XLA Modules:
  0.0 171.3 jit_solution(9452243984679171026)
XLA Ops:
  0.6 3.2 %prelude.1 = (bf16[32,80,256]{2,1,0:T(8,128)(2,1)}, f32[512,128]{1,0:T(8,128)}) custom-call(s32[1]{0:T(128)} %bitcast.11.me_ref, bf16[128,2048]{1,0:T(8,128)(2,1)} %own_ref.1, bf16[128,2048]{1,0:T(8,128)(2,1)} %own_ref.1, s32[2,128]{1,0:T(2,128)} %bitcast.63, f32[2,128]{1,0:T(2,128)} %bitcast.64, f32[64,64,128]{2,1,0:T(8,128)} %down_ref.1), custom_call_target="tpu_custom_call" | custom-call | tf_op jit(solution)/shard_map/prelude/pallas_call | solution.py:110
  3.8 11.3 %all-to-all-start = ((bf16[32,80,256]{2,1,0:T(8,128)(2,1)}), bf16[32,80,256]{2,1,0:T(8,128)(2,1)S(1)}, u32[]{:S(2)}, u32[]{:S(2)}) async-start(bf16[32,80,256]{2,1,0:T(8,128)(2,1)} %get-tuple-element.16), calls=%async_computation | async-start | bytes 2621440 | tf_op jit(solution)/shard_map/all_to_all | solution.py:19
  15.2 3.7 %multiply_convert_fusion.3 = (bf16[32,64,128]{2,1,0:T(8,128)(2,1)}, bf16[32,64,128]{2,1,0:T(8,128)(2,1)}, bf16[32,64,128]{2,1,0:T(8,128)(2,1)}, bf16[32,64,128]{2,1,0:T(8,128)(2,1)S(1)}) fusion(f32[64,64,128]{2,1,0:T(8,128)} %param.11, f32[64]{0:T(128)S(1)} %copy-done.10, f32[64,64,128]{2,1,0:T(8,128)} %param.12), kind=kLoop, calls=%fused_computation.11 | loop fusion | flops 2097152 | bytes 6291712 | tf_op jit(solution)/shard_map/convert_element_type | solution.py:290
  18.9 0.8 copy-done.2
  19.7 2.6 %pad_maximum_fusion.1 = bf16[32,48,512]{2,1,0:T(8,128)(2,1)} fusion(bf16[32,64,128]{2,1,0:T(8,128)(2,1)} %get-tuple-element.46, bf16[32,64,128]{2,1,0:T(8,128)(2,1)} %get-tuple-element.21, bf16[32,64,128]{2,1,0:T(8,128)(2,1)S(1)} %get-tuple-element.47, bf16[32,64,128]{2,1,0:T(8,128)(2,1)} %get-tuple-element.20), kind=kLoop, calls=%fused_computation.1 | loop fusion | flops 6291456 | bytes 3670016 | tf_op jit(solution)/shard_map/concatenate | solution.py:288
  22.3 25.6 %all-to-all-done = bf16[32,80,256]{2,1,0:T(8,128)(2,1)S(1)} async-done(((bf16[32,80,256]{2,1,0:T(8,128)(2,1)}), bf16[32,80,256]{2,1,0:T(8,128)(2,1)S(1)}, u32[]{:S(2)}, u32[]{:S(2)}) %all-to-all-start) | async-done | bytes 1310752 | tf_op jit(solution)/shard_map/all_to_all | solution.py:19
  48.0 6.5 %all-to-all-start.1 = ((bf16[32,48,512]{2,1,0:T(8,128)(2,1)}), bf16[32,48,512]{2,1,0:T(8,128)(2,1)S(1)}, u32[]{:S(2)}, u32[]{:S(2)}) async-start(bf16[32,48,512]{2,1,0:T(8,128)(2,1)} %pad_maximum_fusion.1), calls=%async_computation.1 | async-start | bytes 3145728 | tf_op jit(solution)/shard_map/all_to_all | solution.py:19
  54.6 1.2 pad_maximum_fusion.7
  55.8 0.7 dynamic-slice_bitcast_fusion.8
  56.7 3.9 %collective-permute-start.5 = (bf16[4,16,512]{2,1,0:T(8,128)(2,1)S(1)}, bf16[4,16,512]{2,1,0:T(8,128)(2,1)S(1)}, u32[]{:S(2)}, u32[]{:S(2)}) collective-permute-start(bf16[4,16,512]{2,1,0:T(8,128)(2,1)S(1)} %get-tuple-element.39), channel_id=1, source_target_pairs={{0,192},{8,200},{16,208},{24,216},{32,224},{40,232},{48,240},{56,2... | collective-permute-start | bytes 196616 | tf_op jit(solution)/shard_map/ppermute | solution.py:191
  60.7 2.3 %collective-permute-start.4 = (bf16[4,16,512]{2,1,0:T(8,128)(2,1)S(1)}, bf16[4,16,512]{2,1,0:T(8,128)(2,1)S(1)}, u32[]{:S(2)}, u32[]{:S(2)}) collective-permute-start(bf16[4,16,512]{2,1,0:T(8,128)(2,1)S(1)} %get-tuple-element.40), channel_id=1, source_target_pairs={{0,160},{8,168},{16,176},{24,184},{32,192},{40,200},{48,208},{56,2... | collective-permute-start | bytes 196616 | tf_op jit(solution)/shard_map/ppermute | solution.py:191
  63.0 2.7 %collective-permute-start.3 = (bf16[4,16,512]{2,1,0:T(8,128)(2,1)S(1)}, bf16[4,16,512]{2,1,0:T(8,128)(2,1)S(1)}, u32[]{:S(2)}, u32[]{:S(2)}) collective-permute-start(bf16[4,16,512]{2,1,0:T(8,128)(2,1)S(1)} %get-tuple-element.41), channel_id=1, source_target_pairs={{0,128},{8,136},{16,144},{24,152},{32,160},{40,168},{48,176},{56,1... | collective-permute-start | bytes 196616 | tf_op jit(solution)/shard_map/ppermute | solution.py:191
  65.8 3.1 %collective-permute-start.15 = (bf16[32,16,256]{2,1,0:T(8,128)(2,1)S(1)}, bf16[32,16,256]{2,1,0:T(8,128)(2,1)}, u32[]{:S(2)}, u32[]{:S(2)}) collective-permute-start(bf16[32,16,256]{2,1,0:T(8,128)(2,1)S(1)} %slice.55.refs_0_), channel_id=1, source_target_pairs={{0,6},{1,7},{2,0},{3,1},{4,2},{5,3},{6,4},{7,5},{8,14},{9,15},{10,... | collective-permute-start | bytes 786440 | tf_op jit(solution)/shard_map/ppermute | solution.py:29
  68.8 24.8 %collective-permute-done.6.refs_7_ = bf16[4,16,512]{2,1,0:T(8,128)(2,1)S(1)} collective-permute-done((bf16[4,16,512]{2,1,0:T(8,128)(2,1)S(1)}, bf16[4,16,512]{2,1,0:T(8,128)(2,1)S(1)}, u32[]{:S(2)}, u32[]{:S(2)}) %collective-permute-start.6) | collective-permute-done | bytes 65568 | tf_op jit(solution)/shard_map/ppermute | solution.py:191
  93.6 3.2 %collective-permute-start.13 = (bf16[32,16,256]{2,1,0:T(8,128)(2,1)S(1)}, bf16[32,16,256]{2,1,0:T(8,128)(2,1)}, u32[]{:S(2)}, u32[]{:S(2)}) collective-permute-start(bf16[32,16,256]{2,1,0:T(8,128)(2,1)S(1)} %slice.55.refs_0_), channel_id=1, source_target_pairs={{0,4},{1,5},{2,6},{3,7},{4,0},{5,1},{6,2},{7,3},{8,12},{9,13},{10,... | collective-permute-start | bytes 786440 | tf_op jit(solution)/shard_map/ppermute | solution.py:29
  96.8 2.9 %collective-permute-start.2 = (bf16[4,16,512]{2,1,0:T(8,128)(2,1)}, bf16[4,16,512]{2,1,0:T(8,128)(2,1)S(1)}, u32[]{:S(2)}, u32[]{:S(2)}) collective-permute-start(bf16[4,16,512]{2,1,0:T(8,128)(2,1)} %get-tuple-element.42), channel_id=1, source_target_pairs={{0,96},{8,104},{16,112},{24,120},{32,128},{40,136},{48,144},{56,15... | collective-permute-start | bytes 196616 | tf_op jit(solution)/shard_map/ppermute | solution.py:191
  99.8 1.3 collective-permute-done.4.refs_5_
  101.1 1.8 %collective-permute-start.1 = (bf16[4,16,512]{2,1,0:T(8,128)(2,1)}, bf16[4,16,512]{2,1,0:T(8,128)(2,1)S(1)}, u32[]{:S(2)}, u32[]{:S(2)}) collective-permute-start(bf16[4,16,512]{2,1,0:T(8,128)(2,1)} %get-tuple-element.43), channel_id=1, source_target_pairs={{0,64},{8,72},{16,80},{24,88},{32,96},{40,104},{48,112},{56,120},{... | collective-permute-start | bytes 196616 | tf_op jit(solution)/shard_map/ppermute | solution.py:191
  103.0 1.4 collective-permute-done.2.refs_3_
  104.4 3.7 %collective-permute-done.1.refs_2_ = bf16[4,16,512]{2,1,0:T(8,128)(2,1)S(1)} collective-permute-done((bf16[4,16,512]{2,1,0:T(8,128)(2,1)}, bf16[4,16,512]{2,1,0:T(8,128)(2,1)S(1)}, u32[]{:S(2)}, u32[]{:S(2)}) %collective-permute-start.1) | collective-permute-done | bytes 65568 | tf_op jit(solution)/shard_map/ppermute | solution.py:191
  108.1 1.5 collective-permute-start.7
  109.5 3.5 %collective-permute-start.8 = (bf16[8,16,512]{2,1,0:T(8,128)(2,1)S(1)}, bf16[8,16,512]{2,1,0:T(8,128)(2,1)S(1)}, u32[]{:S(2)}, u32[]{:S(2)}) collective-permute-start(bf16[8,16,512]{2,1,0:T(8,128)(2,1)S(1)} %get-tuple-element.14), channel_id=1, source_target_pairs={{0,16},{8,24},{16,0},{24,8},{32,48},{40,56},{48,32},{56,40},{64,80... | collective-permute-start | bytes 393224 | tf_op jit(solution)/shard_map/ppermute | solution.py:221
  113.1 0.6 collective-permute-start.9
  113.7 0.8 collective-permute-done.7.refs_1_
  114.5 1.6 collective-permute-start.11
  116.1 1.3 collective-permute-done.8.refs_2_
  118.2 1.3 slice.52
  119.5 1.0 dynamic-slice_bitcast_fusion
  120.5 3.0 %collective-permute-start.30 = (bf16[256,256]{1,0:T(8,128)(2,1)}, bf16[256,256]{1,0:T(8,128)(2,1)S(1)}, u32[]{:S(2)}, u32[]{:S(2)}) collective-permute-start(bf16[256,256]{1,0:T(8,128)(2,1)} %get-tuple-element.28), channel_id=1, source_target_pairs={{0,7},{1,6},{2,1},{3,0},{4,3},{5,2},{6,5},{7,4},{8,15},{9,14},{10,... | collective-permute-start | bytes 393224 | tf_op jit(solution)/shard_map/ppermute | solution.py:29
  123.5 0.7 collective-permute-start.29
  124.3 2.9 %collective-permute-start.27 = (bf16[256,256]{1,0:T(8,128)(2,1)}, bf16[256,256]{1,0:T(8,128)(2,1)S(1)}, u32[]{:S(2)}, u32[]{:S(2)}) collective-permute-start(bf16[256,256]{1,0:T(8,128)(2,1)} %get-tuple-element.31), channel_id=1, source_target_pairs={{0,4},{1,5},{2,6},{3,7},{4,0},{5,1},{6,2},{7,3},{8,12},{9,13},{10,... | collective-permute-start | bytes 393224 | tf_op jit(solution)/shard_map/ppermute | solution.py:29
  127.6 0.9 slice_bitcast_fusion.1
  129.0 0.7 copy-done.6
  129.7 1.3 collective-permute-start.26
  131.0 2.7 %hidden_units.1.refs_0_ = bf16[512,128]{1,0:T(8,128)(2,1)S(1)} custom-call(s32[2]{0:T(128)S(1)} %pad_add_fusion.me_ref, bf16[32,16,512]{2,1,0:T(8,128)(2,1)S(1)} %sources_in_order.1.top_ref, bf16[32,48,512]{2,1,0:T(8,128)(2,1)S(1)} %all-to-all-done.1.rest_ref, bf16[32,16,256]{2,1,0:T(8,128)(2,1)} %copy-done.4, bf16[32,16,256]{2,1,0:T(8,128)(2,1)} %copy-done.5, ...), custom_call_target="tpu_custom_call" | custom-call | tf_op jit(solution)/shard_map/hidden_units/pallas_call | solution.py:169
  133.8 1.7 %collective-permute-done.29.refs_14_ = bf16[256,256]{1,0:T(8,128)(2,1)S(1)} collective-permute-done((bf16[256,256]{1,0:T(8,128)(2,1)}, bf16[256,256]{1,0:T(8,128)(2,1)S(1)}, u32[]{:S(2)}, u32[]{:S(2)}) %collective-permute-start.29) | collective-permute-done | bytes 131104 | tf_op jit(solution)/shard_map/ppermute | solution.py:29
  135.5 3.6 %collective-permute-start.22 = (bf16[512,128]{1,0:T(8,128)(2,1)S(1)}, bf16[512,128]{1,0:T(8,128)(2,1)S(1)}, u32[]{:S(2)}, u32[]{:S(2)}) collective-permute-start(bf16[512,128]{1,0:T(8,128)(2,1)S(1)} %hidden_units.1.refs_0_), channel_id=1, source_target_pairs={{0,6},{1,7},{2,0},{3,1},{4,2},{5,3},{6,4},{7,5},{8,14},{9,15},{10,... | collective-permute-start | bytes 393224 | tf_op jit(solution)/shard_map/ppermute | solution.py:29
  139.1 0.9 collective-permute-start.18
  140.0 1.1 pad_maximum_fusion.6
  141.6 2.8 %collective-permute-done.22.refs_6_ = bf16[512,128]{1,0:T(8,128)(2,1)S(1)} collective-permute-done((bf16[512,128]{1,0:T(8,128)(2,1)S(1)}, bf16[512,128]{1,0:T(8,128)(2,1)S(1)}, u32[]{:S(2)}, u32[]{:S(2)}) %collective-permute-start.22) | collective-permute-done | bytes 131104 | tf_op jit(solution)/shard_map/ppermute | solution.py:29
  144.4 2.3 %collective-permute-done.20.refs_4_ = bf16[512,128]{1,0:T(8,128)(2,1)S(1)} collective-permute-done((bf16[512,128]{1,0:T(8,128)(2,1)S(1)}, bf16[512,128]{1,0:T(8,128)(2,1)S(1)}, u32[]{:S(2)}, u32[]{:S(2)}) %collective-permute-start.20) | collective-permute-done | bytes 131104 | tf_op jit(solution)/shard_map/ppermute | solution.py:29
  146.7 1.1 collective-permute-done.18.refs_2_
  147.9 1.5 pad_maximum_fusion
  149.5 1.2 down_projected.1
  150.7 6.8 %all-to-all-start.2 = ((bf16[32,16,256]{2,1,0:T(8,128)(2,1)}), bf16[32,16,256]{2,1,0:T(8,128)(2,1)S(1)}, u32[]{:S(2)}, u32[]{:S(2)}) async-start(bf16[32,16,256]{2,1,0:T(8,128)(2,1)} %down_projected.1), calls=%async_computation.2 | async-start | bytes 524288 | tf_op jit(solution)/shard_map/all_to_all | solution.py:19
  157.9 1.5 pad_maximum_fusion.4
  159.4 10.9 %all-to-all-done.2 = bf16[32,16,256]{2,1,0:T(8,128)(2,1)S(1)} async-done(((bf16[32,16,256]{2,1,0:T(8,128)(2,1)}), bf16[32,16,256]{2,1,0:T(8,128)(2,1)S(1)}, u32[]{:S(2)}, u32[]{:S(2)}) %all-to-all-start.2) | async-done | bytes 262176 | tf_op jit(solution)/shard_map/all_to_all | solution.py:19
  170.3 1.0 convolution_convert_fusion
  (61 shorter events, 3.2 us)
Async XLA Ops:
  3.8 11.3 %copy-start.10 = (f32[64]{0:T(128)S(1)}, f32[64]{0:T(128)}, u32[]{:S(2)}) copy-start(f32[64]{0:T(128)} %param.10) | copy-start | bytes 772
  3.8 44.1 %all-to-all-start = ((bf16[32,80,256]{2,1,0:T(8,128)(2,1)}), bf16[32,80,256]{2,1,0:T(8,128)(2,1)S(1)}, u32[]{:S(2)}, u32[]{:S(2)}) async-start(bf16[32,80,256]{2,1,0:T(8,128)(2,1)} %get-tuple-element.16), calls=%async_computation | async-start | bytes 2621440 | tf_op jit(solution)/shard_map/all_to_all | solution.py:19
  18.9 0.8 copy-start.2
  47.9 48.9 %copy-start.1 = (bf16[32,80,256]{2,1,0:T(8,128)(2,1)}, bf16[32,80,256]{2,1,0:T(8,128)(2,1)S(1)}, u32[]{:S(2)}) copy-start(bf16[32,80,256]{2,1,0:T(8,128)(2,1)S(1)} %all-to-all-done) | copy-start | bytes 3932164
  48.0 83.0 %all-to-all-start.1 = ((bf16[32,48,512]{2,1,0:T(8,128)(2,1)}), bf16[32,48,512]{2,1,0:T(8,128)(2,1)S(1)}, u32[]{:S(2)}, u32[]{:S(2)}) async-start(bf16[32,48,512]{2,1,0:T(8,128)(2,1)} %pad_maximum_fusion.1), calls=%async_computation.1 | async-start | bytes 3145728 | tf_op jit(solution)/shard_map/all_to_all | solution.py:19
  56.5 37.2 %collective-permute-start.6 = (bf16[4,16,512]{2,1,0:T(8,128)(2,1)S(1)}, bf16[4,16,512]{2,1,0:T(8,128)(2,1)S(1)}, u32[]{:S(2)}, u32[]{:S(2)}) collective-permute-start(bf16[4,16,512]{2,1,0:T(8,128)(2,1)S(1)} %get-tuple-element.38), channel_id=1, source_target_pairs={{0,224},{8,232},{16,240},{24,248},{32,0},{40,8},{48,16},{56,24},{6... | collective-permute-start | bytes 196616 | tf_op jit(solution)/shard_map/ppermute | solution.py:191
  56.7 40.1 %collective-permute-start.5 = (bf16[4,16,512]{2,1,0:T(8,128)(2,1)S(1)}, bf16[4,16,512]{2,1,0:T(8,128)(2,1)S(1)}, u32[]{:S(2)}, u32[]{:S(2)}) collective-permute-start(bf16[4,16,512]{2,1,0:T(8,128)(2,1)S(1)} %get-tuple-element.39), channel_id=1, source_target_pairs={{0,192},{8,200},{16,208},{24,216},{32,224},{40,232},{48,240},{56,2... | collective-permute-start | bytes 196616 | tf_op jit(solution)/shard_map/ppermute | solution.py:191
  60.7 40.4 %collective-permute-start.4 = (bf16[4,16,512]{2,1,0:T(8,128)(2,1)S(1)}, bf16[4,16,512]{2,1,0:T(8,128)(2,1)S(1)}, u32[]{:S(2)}, u32[]{:S(2)}) collective-permute-start(bf16[4,16,512]{2,1,0:T(8,128)(2,1)S(1)} %get-tuple-element.40), channel_id=1, source_target_pairs={{0,160},{8,168},{16,176},{24,184},{32,192},{40,200},{48,208},{56,2... | collective-permute-start | bytes 196616 | tf_op jit(solution)/shard_map/ppermute | solution.py:191
  63.0 40.0 %collective-permute-start.3 = (bf16[4,16,512]{2,1,0:T(8,128)(2,1)S(1)}, bf16[4,16,512]{2,1,0:T(8,128)(2,1)S(1)}, u32[]{:S(2)}, u32[]{:S(2)}) collective-permute-start(bf16[4,16,512]{2,1,0:T(8,128)(2,1)S(1)} %get-tuple-element.41), channel_id=1, source_target_pairs={{0,128},{8,136},{16,144},{24,152},{32,160},{40,168},{48,176},{56,1... | collective-permute-start | bytes 196616 | tf_op jit(solution)/shard_map/ppermute | solution.py:191
  65.7 54.7 %copy-start.4 = (bf16[32,16,256]{2,1,0:T(8,128)(2,1)}, bf16[32,16,256]{2,1,0:T(8,128)(2,1)S(1)}, u32[]{:S(2)}) copy-start(bf16[32,16,256]{2,1,0:T(8,128)(2,1)S(1)} %slice.55.refs_0_) | copy-start | bytes 786436
  65.8 51.6 %collective-permute-start.15 = (bf16[32,16,256]{2,1,0:T(8,128)(2,1)S(1)}, bf16[32,16,256]{2,1,0:T(8,128)(2,1)}, u32[]{:S(2)}, u32[]{:S(2)}) collective-permute-start(bf16[32,16,256]{2,1,0:T(8,128)(2,1)S(1)} %slice.55.refs_0_), channel_id=1, source_target_pairs={{0,6},{1,7},{2,0},{3,1},{4,2},{5,3},{6,4},{7,5},{8,14},{9,15},{10,... | collective-permute-start | bytes 786440 | tf_op jit(solution)/shard_map/ppermute | solution.py:29
  93.6 24.3 %collective-permute-start.13 = (bf16[32,16,256]{2,1,0:T(8,128)(2,1)S(1)}, bf16[32,16,256]{2,1,0:T(8,128)(2,1)}, u32[]{:S(2)}, u32[]{:S(2)}) collective-permute-start(bf16[32,16,256]{2,1,0:T(8,128)(2,1)S(1)} %slice.55.refs_0_), channel_id=1, source_target_pairs={{0,4},{1,5},{2,6},{3,7},{4,0},{5,1},{6,2},{7,3},{8,12},{9,13},{10,... | collective-permute-start | bytes 786440 | tf_op jit(solution)/shard_map/ppermute | solution.py:29
  96.8 7.5 %collective-permute-start.2 = (bf16[4,16,512]{2,1,0:T(8,128)(2,1)}, bf16[4,16,512]{2,1,0:T(8,128)(2,1)S(1)}, u32[]{:S(2)}, u32[]{:S(2)}) collective-permute-start(bf16[4,16,512]{2,1,0:T(8,128)(2,1)} %get-tuple-element.42), channel_id=1, source_target_pairs={{0,96},{8,104},{16,112},{24,120},{32,128},{40,136},{48,144},{56,15... | collective-permute-start | bytes 196616 | tf_op jit(solution)/shard_map/ppermute | solution.py:191
  101.1 7.0 %collective-permute-start.1 = (bf16[4,16,512]{2,1,0:T(8,128)(2,1)}, bf16[4,16,512]{2,1,0:T(8,128)(2,1)S(1)}, u32[]{:S(2)}, u32[]{:S(2)}) collective-permute-start(bf16[4,16,512]{2,1,0:T(8,128)(2,1)} %get-tuple-element.43), channel_id=1, source_target_pairs={{0,64},{8,72},{16,80},{24,88},{32,96},{40,104},{48,112},{56,120},{... | collective-permute-start | bytes 196616 | tf_op jit(solution)/shard_map/ppermute | solution.py:191
  103.0 5.1 %collective-permute-start = (bf16[4,16,512]{2,1,0:T(8,128)(2,1)S(1)}, bf16[4,16,512]{2,1,0:T(8,128)(2,1)S(1)}, u32[]{:S(2)}, u32[]{:S(2)}) collective-permute-start(bf16[4,16,512]{2,1,0:T(8,128)(2,1)S(1)} %get-tuple-element.44), channel_id=1, source_target_pairs={{0,32},{8,40},{16,48},{24,56},{32,64},{40,72},{48,80},{56,88},{64,... | collective-permute-start | bytes 196616 | tf_op jit(solution)/shard_map/ppermute | solution.py:191
  108.1 6.4 %collective-permute-start.7 = (bf16[8,16,512]{2,1,0:T(8,128)(2,1)S(1)}, bf16[8,16,512]{2,1,0:T(8,128)(2,1)S(1)}, u32[]{:S(2)}, u32[]{:S(2)}) collective-permute-start(bf16[8,16,512]{2,1,0:T(8,128)(2,1)S(1)} %get-tuple-element.13), channel_id=1, source_target_pairs={{0,8},{8,16},{16,24},{24,0},{32,40},{40,48},{48,56},{56,32},{64,72... | collective-permute-start | bytes 393224 | tf_op jit(solution)/shard_map/ppermute | solution.py:221
  109.5 7.8 %collective-permute-start.8 = (bf16[8,16,512]{2,1,0:T(8,128)(2,1)S(1)}, bf16[8,16,512]{2,1,0:T(8,128)(2,1)S(1)}, u32[]{:S(2)}, u32[]{:S(2)}) collective-permute-start(bf16[8,16,512]{2,1,0:T(8,128)(2,1)S(1)} %get-tuple-element.14), channel_id=1, source_target_pairs={{0,16},{8,24},{16,0},{24,8},{32,48},{40,56},{48,32},{56,40},{64,80... | collective-permute-start | bytes 393224 | tf_op jit(solution)/shard_map/ppermute | solution.py:221
  113.1 5.0 %collective-permute-start.9 = (bf16[8,16,512]{2,1,0:T(8,128)(2,1)S(1)}, bf16[8,16,512]{2,1,0:T(8,128)(2,1)S(1)}, u32[]{:S(2)}, u32[]{:S(2)}) collective-permute-start(bf16[8,16,512]{2,1,0:T(8,128)(2,1)S(1)} %get-tuple-element.15), channel_id=1, source_target_pairs={{0,24},{8,0},{16,8},{24,16},{32,56},{40,32},{48,40},{56,48},{64,88... | collective-permute-start | bytes 393224 | tf_op jit(solution)/shard_map/ppermute | solution.py:221
  114.5 9.0 %collective-permute-start.11 = (bf16[32,16,256]{2,1,0:T(8,128)(2,1)S(1)}, bf16[32,16,256]{2,1,0:T(8,128)(2,1)}, u32[]{:S(2)}, u32[]{:S(2)}) collective-permute-start(bf16[32,16,256]{2,1,0:T(8,128)(2,1)S(1)} %slice.55.refs_0_), channel_id=1, source_target_pairs={{0,2},{1,3},{2,4},{3,5},{4,6},{5,7},{6,0},{7,1},{8,10},{9,11},{10,... | collective-permute-start | bytes 786440 | tf_op jit(solution)/shard_map/ppermute | solution.py:29
  117.4 6.9 %collective-permute-start.10 = (bf16[32,16,256]{2,1,0:T(8,128)(2,1)S(1)}, bf16[32,16,256]{2,1,0:T(8,128)(2,1)S(1)}, u32[]{:S(2)}, u32[]{:S(2)}) collective-permute-start(bf16[32,16,256]{2,1,0:T(8,128)(2,1)S(1)} %slice.55.refs_0_), channel_id=1, source_target_pairs={{0,1},{1,0},{2,3},{3,2},{4,5},{5,4},{6,7},{7,6},{8,9},{9,8},{10,11... | collective-permute-start | bytes 786440 | tf_op jit(solution)/shard_map/ppermute | solution.py:29
  117.4 6.9 %collective-permute-start.16 = (bf16[32,16,256]{2,1,0:T(8,128)(2,1)}, bf16[32,16,256]{2,1,0:T(8,128)(2,1)}, u32[]{:S(2)}, u32[]{:S(2)}) collective-permute-start(bf16[32,16,256]{2,1,0:T(8,128)(2,1)} %collective-permute-done.15.refs_6_), channel_id=1, source_target_pairs={{0,1},{1,0},{2,3},{3,2},{4,5},{5,4},{6,7},{7,6},{8,9},{9,8},{10,11... | collective-permute-start | bytes 786440 | tf_op jit(solution)/shard_map/ppermute | solution.py:29
  117.9 9.3 %collective-permute-start.14 = (bf16[32,16,256]{2,1,0:T(8,128)(2,1)}, bf16[32,16,256]{2,1,0:T(8,128)(2,1)}, u32[]{:S(2)}, u32[]{:S(2)}) collective-permute-start(bf16[32,16,256]{2,1,0:T(8,128)(2,1)} %collective-permute-done.13.refs_4_), channel_id=1, source_target_pairs={{0,1},{1,0},{2,3},{3,2},{4,5},{5,4},{6,7},{7,6},{8,9},{9,8},{10,11... | collective-permute-start | bytes 786440 | tf_op jit(solution)/shard_map/ppermute | solution.py:29
  120.5 13.2 %collective-permute-start.30 = (bf16[256,256]{1,0:T(8,128)(2,1)}, bf16[256,256]{1,0:T(8,128)(2,1)S(1)}, u32[]{:S(2)}, u32[]{:S(2)}) collective-permute-start(bf16[256,256]{1,0:T(8,128)(2,1)} %get-tuple-element.28), channel_id=1, source_target_pairs={{0,7},{1,6},{2,1},{3,0},{4,3},{5,2},{6,5},{7,4},{8,15},{9,14},{10,... | collective-permute-start | bytes 393224 | tf_op jit(solution)/shard_map/ppermute | solution.py:29
  123.5 12.0 %collective-permute-start.29 = (bf16[256,256]{1,0:T(8,128)(2,1)}, bf16[256,256]{1,0:T(8,128)(2,1)S(1)}, u32[]{:S(2)}, u32[]{:S(2)}) collective-permute-start(bf16[256,256]{1,0:T(8,128)(2,1)} %get-tuple-element.29), channel_id=1, source_target_pairs={{0,6},{1,7},{2,0},{3,1},{4,2},{5,3},{6,4},{7,5},{8,14},{9,15},{10,... | collective-permute-start | bytes 393224 | tf_op jit(solution)/shard_map/ppermute | solution.py:29
  124.3 3.4 %copy-start.5 = (bf16[32,16,256]{2,1,0:T(8,128)(2,1)}, bf16[32,16,256]{2,1,0:T(8,128)(2,1)S(1)}, u32[]{:S(2)}) copy-start(bf16[32,16,256]{2,1,0:T(8,128)(2,1)S(1)} %collective-permute-done.10.refs_1_) | copy-start | bytes 786436
  124.3 14.9 %collective-permute-start.28 = (bf16[256,256]{1,0:T(8,128)(2,1)}, bf16[256,256]{1,0:T(8,128)(2,1)S(1)}, u32[]{:S(2)}, u32[]{:S(2)}) collective-permute-start(bf16[256,256]{1,0:T(8,128)(2,1)} %get-tuple-element.30), channel_id=1, source_target_pairs={{0,5},{1,4},{2,7},{3,6},{4,1},{5,0},{6,3},{7,2},{8,13},{9,12},{10,... | collective-permute-start | bytes 393224 | tf_op jit(solution)/shard_map/ppermute | solution.py:29
  124.3 14.9 %collective-permute-start.27 = (bf16[256,256]{1,0:T(8,128)(2,1)}, bf16[256,256]{1,0:T(8,128)(2,1)S(1)}, u32[]{:S(2)}, u32[]{:S(2)}) collective-permute-start(bf16[256,256]{1,0:T(8,128)(2,1)} %get-tuple-element.31), channel_id=1, source_target_pairs={{0,4},{1,5},{2,6},{3,7},{4,0},{5,1},{6,2},{7,3},{8,12},{9,13},{10,... | collective-permute-start | bytes 393224 | tf_op jit(solution)/shard_map/ppermute | solution.py:29
  127.2 1.8 %collective-permute-start.12 = (bf16[32,16,256]{2,1,0:T(8,128)(2,1)}, bf16[32,16,256]{2,1,0:T(8,128)(2,1)S(1)}, u32[]{:S(2)}, u32[]{:S(2)}) collective-permute-start(bf16[32,16,256]{2,1,0:T(8,128)(2,1)} %collective-permute-done.11.refs_2_), channel_id=1, source_target_pairs={{0,1},{1,0},{2,3},{3,2},{4,5},{5,4},{6,7},{7,6},{8,9},{9,8},{10,11... | collective-permute-start | bytes 786440 | tf_op jit(solution)/shard_map/ppermute | solution.py:29
  129.0 0.7 copy-start.6
  129.7 4.0 %copy-start.9 = (bf16[256,256]{1,0:T(8,128)(2,1)S(1)}, bf16[256,256]{1,0:T(8,128)(2,1)}, u32[]{:S(2)}) copy-start(bf16[256,256]{1,0:T(8,128)(2,1)} %get-tuple-element.33) | copy-start | bytes 393220
  129.7 11.3 %collective-permute-start.26 = (bf16[256,256]{1,0:T(8,128)(2,1)}, bf16[256,256]{1,0:T(8,128)(2,1)S(1)}, u32[]{:S(2)}, u32[]{:S(2)}) collective-permute-start(bf16[256,256]{1,0:T(8,128)(2,1)} %get-tuple-element.32), channel_id=1, source_target_pairs={{0,3},{1,2},{2,5},{3,4},{4,7},{5,6},{6,1},{7,0},{8,11},{9,10},{10,... | collective-permute-start | bytes 393224 | tf_op jit(solution)/shard_map/ppermute | solution.py:29
  131.0 9.0 %copy-start.3 = (bf16[1,2048,128]{2,1,0:T(8,128)(2,1)S(1)}, bf16[1,2048,128]{2,1,0:T(8,128)(2,1)}, u32[]{:S(2)}) copy-start(bf16[1,2048,128]{2,1,0:T(8,128)(2,1)} %get-tuple-element.37) | copy-start | bytes 1572868
  133.7 7.4 %copy-start.8 = (bf16[256,256]{1,0:T(8,128)(2,1)S(1)}, bf16[256,256]{1,0:T(8,128)(2,1)}, u32[]{:S(2)}) copy-start(bf16[256,256]{1,0:T(8,128)(2,1)} %get-tuple-element.34) | copy-start | bytes 393220
  133.7 7.4 %collective-permute-start.25 = (bf16[256,256]{1,0:T(8,128)(2,1)S(1)}, bf16[256,256]{1,0:T(8,128)(2,1)S(1)}, u32[]{:S(2)}, u32[]{:S(2)}) collective-permute-start(bf16[256,256]{1,0:T(8,128)(2,1)S(1)} %copy-done.9), channel_id=1, source_target_pairs={{0,2},{1,3},{2,4},{3,5},{4,6},{5,7},{6,0},{7,1},{8,10},{9,11},{10,... | collective-permute-start | bytes 393224 | tf_op jit(solution)/shard_map/ppermute | solution.py:29
  135.5 8.8 %collective-permute-start.22 = (bf16[512,128]{1,0:T(8,128)(2,1)S(1)}, bf16[512,128]{1,0:T(8,128)(2,1)S(1)}, u32[]{:S(2)}, u32[]{:S(2)}) collective-permute-start(bf16[512,128]{1,0:T(8,128)(2,1)S(1)} %hidden_units.1.refs_0_), channel_id=1, source_target_pairs={{0,6},{1,7},{2,0},{3,1},{4,2},{5,3},{6,4},{7,5},{8,14},{9,15},{10,... | collective-permute-start | bytes 393224 | tf_op jit(solution)/shard_map/ppermute | solution.py:29
  139.1 7.6 %collective-permute-start.20 = (bf16[512,128]{1,0:T(8,128)(2,1)S(1)}, bf16[512,128]{1,0:T(8,128)(2,1)S(1)}, u32[]{:S(2)}, u32[]{:S(2)}) collective-permute-start(bf16[512,128]{1,0:T(8,128)(2,1)S(1)} %hidden_units.1.refs_0_), channel_id=1, source_target_pairs={{0,4},{1,5},{2,6},{3,7},{4,0},{5,1},{6,2},{7,3},{8,12},{9,13},{10,... | collective-permute-start | bytes 393224 | tf_op jit(solution)/shard_map/ppermute | solution.py:29
  139.1 8.7 %collective-permute-start.18 = (bf16[512,128]{1,0:T(8,128)(2,1)S(1)}, bf16[512,128]{1,0:T(8,128)(2,1)S(1)}, u32[]{:S(2)}, u32[]{:S(2)}) collective-permute-start(bf16[512,128]{1,0:T(8,128)(2,1)S(1)} %hidden_units.1.refs_0_), channel_id=1, source_target_pairs={{0,2},{1,3},{2,4},{3,5},{4,6},{5,7},{6,0},{7,1},{8,10},{9,11},{10,... | collective-permute-start | bytes 393224 | tf_op jit(solution)/shard_map/ppermute | solution.py:29
  141.1 8.3 %collective-permute-start.24 = (bf16[256,256]{1,0:T(8,128)(2,1)S(1)}, bf16[256,256]{1,0:T(8,128)(2,1)S(1)}, u32[]{:S(2)}, u32[]{:S(2)}) collective-permute-start(bf16[256,256]{1,0:T(8,128)(2,1)S(1)} %copy-done.8), channel_id=1, source_target_pairs={{0,1},{1,0},{2,3},{3,2},{4,5},{5,4},{6,7},{7,6},{8,9},{9,8},{10,11... | collective-permute-start | bytes 393224 | tf_op jit(solution)/shard_map/ppermute | solution.py:29
  141.1 8.3 %collective-permute-start.17 = (bf16[512,128]{1,0:T(8,128)(2,1)S(1)}, bf16[512,128]{1,0:T(8,128)(2,1)S(1)}, u32[]{:S(2)}, u32[]{:S(2)}) collective-permute-start(bf16[512,128]{1,0:T(8,128)(2,1)S(1)} %hidden_units.1.refs_0_), channel_id=1, source_target_pairs={{0,1},{1,0},{2,3},{3,2},{4,5},{5,4},{6,7},{7,6},{8,9},{9,8},{10,11... | collective-permute-start | bytes 393224 | tf_op jit(solution)/shard_map/ppermute | solution.py:29
  144.4 5.1 %collective-permute-start.23 = (bf16[512,128]{1,0:T(8,128)(2,1)S(1)}, bf16[512,128]{1,0:T(8,128)(2,1)S(1)}, u32[]{:S(2)}, u32[]{:S(2)}) collective-permute-start(bf16[512,128]{1,0:T(8,128)(2,1)S(1)} %collective-permute-done.22.refs_6_), channel_id=1, source_target_pairs={{0,1},{1,0},{2,3},{3,2},{4,5},{5,4},{6,7},{7,6},{8,9},{9,8},{10,11... | collective-permute-start | bytes 393224 | tf_op jit(solution)/shard_map/ppermute | solution.py:29
  146.7 2.7 %collective-permute-start.21 = (bf16[512,128]{1,0:T(8,128)(2,1)S(1)}, bf16[512,128]{1,0:T(8,128)(2,1)S(1)}, u32[]{:S(2)}, u32[]{:S(2)}) collective-permute-start(bf16[512,128]{1,0:T(8,128)(2,1)S(1)} %collective-permute-done.20.refs_4_), channel_id=1, source_target_pairs={{0,1},{1,0},{2,3},{3,2},{4,5},{5,4},{6,7},{7,6},{8,9},{9,8},{10,11... | collective-permute-start | bytes 393224 | tf_op jit(solution)/shard_map/ppermute | solution.py:29
  147.9 1.6 collective-permute-start.19
  149.4 8.1 %copy-start = (bf16[32,64,512]{2,1,0:T(8,128)(2,1)S(1)}, bf16[32,64,512]{2,1,0:T(8,128)(2,1)}, u32[]{:S(2)}) copy-start(bf16[32,64,512]{2,1,0:T(8,128)(2,1)} %pad_maximum_fusion) | copy-start | bytes 6291460
  150.7 19.6 %all-to-all-start.2 = ((bf16[32,16,256]{2,1,0:T(8,128)(2,1)}), bf16[32,16,256]{2,1,0:T(8,128)(2,1)S(1)}, u32[]{:S(2)}, u32[]{:S(2)}) async-start(bf16[32,16,256]{2,1,0:T(8,128)(2,1)} %down_projected.1), calls=%async_computation.2 | async-start | bytes 524288 | tf_op jit(solution)/shard_map/all_to_all | solution.py:19
  157.9 12.4 %copy-start.7 = (f32[512,128]{1,0:T(8,128)S(1)}, f32[512,128]{1,0:T(8,128)}, u32[]{:S(2)}) copy-start(f32[512,128]{1,0:T(8,128)} %get-tuple-element.19) | copy-start | bytes 786436
